TPU v7x, 256 devices: a whole 4x4x8 slice. The times are simulated.
256 devices in a mesh: sp: 32 (over z, y), tp: 8 (over x, core).
Axes of the slice: x: 4, y: 4, z: 8, core: 2. Of those that a mesh axis runs over, the one named last changes fastest.
Arguments:
- tokens: bfloat16 [32768, 2048], P('sp'), may hold values from -6 to 6
- in_gain: float32 [2048], replicated, may hold values from 0.1 to 1.9
- w_query: bfloat16 [2048, 1024], P(None, 'tp'), may hold values from -0.125 to 0.125
- w_forget: bfloat16 [2048, 1024], P(None, 'tp'), may hold values from -0.125 to 0.125
- w_input: bfloat16 [2048, 1024], P(None, 'tp'), may hold values from -0.125 to 0.125
- w_outgate: bfloat16 [2048, 1024], P(None, 'tp'), may hold values from -0.125 to 0.125
- w_conv_h: bfloat16 [2048, 1024], P(None, 'tp'), may hold values from -0.125 to 0.125
- w_conv_b: bfloat16 [2048, 1024], P(None, 'tp'), may hold values from -0.125 to 0.125
- w_conv_c: bfloat16 [2048, 1024], P(None, 'tp'), may hold values from -0.125 to 0.125
- forget_floor: float32 [1024], P('tp'), may hold values from 0.84 to 1
- forget_leak: float32 [32768, 1024], P('sp', 'tp'), may hold values from -1 to 0
- state_gain: float32 [128], replicated, may hold values from 0.1 to 1.9
- conv_taps: bfloat16 [3, 1024], P(None, 'tp'), may hold values from -3.5 to 3.5
- group_gain: float32 [128], replicated, may hold values from 0.1 to 1.9
- out_state: bfloat16 [1024, 2048], P('tp'), may hold values from -0.1875 to 0.1875
- out_conv: bfloat16 [1024, 2048], P('tp'), may hold values from -0.1875 to 0.1875
Outputs:
- mixed_out: bfloat16 [32768, 2048], P('sp', 'tp')
All inputs are finite; a program needn't handle non-finite values.
Results may differ from a plain program's by a relative error of at most 0.015.
Values may be sent and summed in bfloat16 or wider, within the bound.
A program may use at most 128 MiB of HBM per device.

v0:
```python
import jax
import jax.numpy as jnp
from jax import lax
from jax.sharding import Mesh
from jax.sharding import PartitionSpec as P

GROUP_FEATURES = 128
BLOCK = 64
TAPS = 3
SP = ("sp_0", "sp_1")


norm_eps = 1e-06


def from_behind(array, axis, by):
    count = lax.axis_size(axis)
    pairs = [(i, i + by) for i in range(count) if 0 <= i + by < count]
    return lax.ppermute(array, axis, pairs)


def neutral_like(array, identity):
    return jax.tree.map(
        lambda part, zero: jnp.zeros_like(part) + jnp.asarray(zero, part.dtype), array, identity
    )


def collected_together(array, axis):
    leaves = jax.tree.leaves(array)
    turns = sorted(range(len(leaves)), key=lambda k: -leaves[k].size)
    width = (1, *leaves[turns[0]].shape)[-1]
    lines = [
        jnp.pad(leaves[k].reshape(-1), (0, -leaves[k].size % width)).reshape(-1, width)
        for k in turns
    ]
    both, at, found = (lax.all_gather(jnp.concatenate(lines), axis), 0, {})
    for k, line in zip(turns, lines):
        section = both[:, at : at + len(line)].reshape(len(both), -1)
        found[k] = section[:, : leaves[k].size].reshape(-1, *leaves[k].shape)
        at += len(line)
    numbers = iter(range(len(leaves)))
    return jax.tree.map(lambda _: found[next(numbers)], array)


def carried_in(array, axes, combine, identity):
    before = start = neutral_like(array, identity)
    subtotal = array
    for axis in reversed(axes):
        count, index = (lax.axis_size(axis), lax.axis_index(axis))
        pieces = collected_together(
            jax.tree.map(
                lambda part, kind: part.astype(kind), subtotal, (jnp.bfloat16, jnp.bfloat16)
            ),
            axis,
        )
        inside, subtotal = (start, start)
        for k in range(count):
            passed = k < index
            subtotal = combine(
                subtotal, jax.tree.map(lambda part, own: part[k].astype(own.dtype), pieces, array)
            )
            inside = jax.tree.map(lambda new, old: jnp.where(passed, new, old), subtotal, inside)
        before = combine(inside, before)
    return before


def rms_rows(values, gain):
    scale = lax.rsqrt(jnp.mean(values * values, axis=-1, keepdims=True) + norm_eps)
    return values * scale * gain


def state_block(carry, inputs):
    carry_state, offset = carry
    query_blk, key_blk, value_blk, logf_blk = inputs
    cum_log = jnp.cumsum(logf_blk, axis=1)
    carried = jnp.einsum("hcd,hde->hce", query_blk * jnp.exp(cum_log), carry_state)
    length = logf_blk.shape[1]
    causal = (jnp.arange(length)[:, None] >= jnp.arange(length)[None, :])[None, :, :, None]
    diff_log = cum_log[:, :, None, :] - cum_log[:, None, :, :]
    decay_all = jnp.exp(jnp.where(causal, diff_log, -jnp.inf))
    scores = jnp.einsum("hid,hjd,hijd->hij", query_blk, key_blk, decay_all)
    result = carried + jnp.einsum("hij,hje->hie", scores, value_blk)
    last_log = cum_log[:, -1, :]
    fresh = jnp.einsum("hcd,hce->hde", key_blk * jnp.exp(last_log[:, None, :] - cum_log), value_blk)
    new_state = jnp.exp(last_log)[:, :, None] * carry_state + fresh
    return ((new_state, offset + last_log), (result, offset[:, None, :] + cum_log))


def join_states(earlier, later):
    earlier_log, earlier_state = earlier
    later_log, later_state = later
    return (earlier_log + later_log, jnp.exp(later_log)[:, :, None] * earlier_state + later_state)


def body(
    tokens,
    in_gain,
    w_query,
    w_forget,
    w_input,
    w_outgate,
    w_conv_h,
    w_conv_b,
    w_conv_c,
    forget_floor,
    forget_leak,
    state_gain,
    conv_taps,
    group_gain,
    out_state,
    out_conv,
):
    count = tokens.shape[0]
    heads = w_query.shape[1] // GROUP_FEATURES
    channels = w_conv_h.shape[1]
    normed = rms_rows(tokens.astype(jnp.float32), in_gain).astype(jnp.bfloat16)

    def project(weight):
        return jnp.dot(normed, weight, preferred_element_type=jnp.float32).astype(jnp.bfloat16)

    proj_query = project(w_query)
    proj_forget = project(w_forget)
    proj_input = project(w_input)
    proj_outgate = project(w_outgate)
    proj_h = project(w_conv_h)
    proj_b = project(w_conv_b)
    proj_c = project(w_conv_c)
    conv_in = (proj_c.astype(jnp.float32) * proj_h.astype(jnp.float32)).astype(jnp.bfloat16)
    rim_rows = from_behind(conv_in[count - (TAPS - 1) :], SP, 1)
    gate_logit = proj_forget.astype(jnp.float32)
    log_forget = (
        jnp.logaddexp(
            jnp.log(forget_floor), jnp.log1p(-forget_floor) + jax.nn.log_sigmoid(gate_logit)
        )
        + forget_leak
    )
    key_gate = (1.0 - forget_floor) * jax.nn.sigmoid(-gate_logit)
    query_act = jax.nn.silu(proj_query.astype(jnp.float32))
    value_f = proj_input.astype(jnp.float32)
    nblk = count // BLOCK

    def to_blocks(arr):
        return arr.reshape(nblk, BLOCK, heads, GROUP_FEATURES).transpose(0, 2, 1, 3)

    def from_blocks(arr):
        return arr.transpose(0, 2, 1, 3).reshape(count, heads, GROUP_FEATURES)

    start_state = jnp.zeros((heads, GROUP_FEATURES, GROUP_FEATURES), jnp.float32)
    start_log = jnp.zeros((heads, GROUP_FEATURES), jnp.float32)
    (local_state, total_log), (local_read, cum_blocks) = lax.scan(
        state_block,
        (start_state, start_log),
        (to_blocks(query_act), to_blocks(key_gate), to_blocks(value_f), to_blocks(log_forget)),
    )
    _, incoming = carried_in((total_log, local_state), SP, join_states, (start_log, start_state))
    cum_device = from_blocks(cum_blocks)
    query_heads = query_act.reshape(count, heads, GROUP_FEATURES)
    cross = jnp.einsum("thd,hde->the", query_heads * jnp.exp(cum_device), incoming)
    state_read = from_blocks(local_read) + cross
    out_gate = jax.nn.silu(proj_outgate.astype(jnp.float32)).reshape(count, heads, GROUP_FEATURES)
    state_res = (
        (rms_rows(state_read, state_gain) * out_gate)
        .reshape(count, heads * GROUP_FEATURES)
        .astype(jnp.bfloat16)
    )
    padded = jnp.concatenate([rim_rows, conv_in], axis=0).astype(jnp.float32)
    taps_f = conv_taps.astype(jnp.float32)
    conv_sum = jnp.zeros((count, channels), jnp.float32)
    for offset in range(TAPS):
        conv_sum = conv_sum + taps_f[offset][None, :] * padded[offset : offset + count]
    gated = (proj_b.astype(jnp.float32) * conv_sum).reshape(
        count, channels // GROUP_FEATURES, GROUP_FEATURES
    )
    conv_res = rms_rows(gated, group_gain).reshape(count, channels).astype(jnp.bfloat16)
    mixed_here = jnp.concatenate([state_res, conv_res], axis=1)
    weight_rows = jnp.concatenate([out_state, out_conv], axis=0)
    columns = lax.all_to_all(weight_rows, "tp", split_axis=1, concat_axis=0, tiled=True)
    summed = jnp.dot(
        lax.all_gather(mixed_here, "tp", axis=1, tiled=True),
        columns,
        preferred_element_type=jnp.float32,
    )
    return summed.astype(jnp.bfloat16)


def solution(mesh):
    split = Mesh(mesh.devices.reshape(8, 4, mesh.shape["tp"]), ("sp_0", "sp_1", "tp"))
    placed = (
        P(SP, None),
        P(),
        P(None, "tp"),
        P(None, "tp"),
        P(None, "tp"),
        P(None, "tp"),
        P(None, "tp"),
        P(None, "tp"),
        P(None, "tp"),
        P("tp"),
        P(SP, "tp"),
        P(),
        P(None, "tp"),
        P(),
        P("tp", None),
        P("tp", None),
    )
    return jax.shard_map(body, mesh=split, in_specs=placed, out_specs=P(SP, "tp"), check_vma=False)
```

profile of v0, /device:TPU:33, one launch (start us, length us, event | category | flops | bytes accessed | tf_op | source)
XLA Modules:
  0.0 185.5 jit_solution(12285283551542501446)
XLA Ops:
  6.5 3.2 %fusion.30 = f32[1024]{0:T(1024)S(1)} fusion(bf16[1024,2048]{1,0:T(8,128)(2,1)} %param.18), kind=kLoop, calls=%fused_computation.44 | loop fusion | flops 6290432 | bytes 4198400 | tf_op jit(solution)/shard_map/reduce_sum | solution.py:68
  11.1 1.2 fusion.37
  12.5 1.3 fusion.36
  13.8 3.2 %collective-permute-start = (bf16[2,128]{1,0:T(2,128)(2,1)S(1)}, bf16[2,128]{1,0:T(2,128)(2,1)S(1)}, u32[]{:S(2)}, u32[]{:S(2)}) collective-permute-start(bf16[2,128]{1,0:T(2,128)(2,1)S(1)} %slice.193), channel_id=1, source_target_pairs={{0,8},{8,16},{16,24},{24,32},{32,40},{40,48},{48,56},{56,64},{64,7... | collective-permute-start | bytes 1544 | tf_op jit(solution)/shard_map/ppermute | solution.py:19
  17.2 3.6 %divide_multiply_fusion = f32[1024,128]{1,0:T(8,128)S(1)} fusion(bf16[1024,2048]{1,0:T(8,128)(2,1)} %copy-done.1, bf16[2048,128]{1,0:T(8,128)(2,1)S(1)} %copy-done.13), kind=kOutput, calls=%fused_computation.83 | convolution fusion | flops 537657344 | bytes 5242880 | tf_op jit(solution)/shard_map/dot_general | solution.py:119
  20.8 1.2 convolution_convert_fusion.6
  22.1 1.8 divide_multiply_fusion.1
  23.8 58.7 %while.17 = (s32[]{:T(128)}, f32[1,128,128]{2,1,0:T(8,128)S(1)}, f32[1,128]{1,0:T(1,128)S(1)}, f32[16,1,64,128]{3,2,1,0:T(8,128)}, f32[16,1,64,128]{3,2,1,0:T(8,...) while((s32[]{:T(128)}, f32[1,128,128]{2,1,0:T(8,128)S(1)}, ...), condition=%wide.region_3.4_spmd.clone, body=%wide.region_1.3_spmd.clone.sunk | while | flops 8487171 | bytes 5119637 | solution.py:150
  24.6 1.7 fusion.189
  28.3 1.7 fusion.189
  32.0 1.7 fusion.189
  35.6 1.7 fusion.189
  39.3 1.7 fusion.189
  43.0 1.7 fusion.189
  46.6 1.7 fusion.189
  50.3 1.7 fusion.189
  54.0 1.7 fusion.189
  57.6 1.7 fusion.189
  61.3 1.7 fusion.189
  65.0 1.7 fusion.189
  68.6 1.7 fusion.189
  72.3 1.7 fusion.189
  76.0 1.7 fusion.189
  79.6 1.7 fusion.189
  82.6 9.5 %all-gather.2 = bf16[4,129,128]{2,1,0:T(8,128)(2,1)S(1)} all-gather(bf16[1,129,128]{2,1,0:T(8,128)(2,1)S(1)} %maximum_bitcast_fusion), channel_id=2, replica_groups=mesh['sp_0'=8,'sp_1'=4,'tp'=8] {'sp_1'}, dimensions={0}, use_global_device_ids=true | all-gather | bytes 165120 | tf_op jit(solution)/shard_map/all_gather | solution.py:36
  92.3 21.4 %all-gather.3 = bf16[8,129,128]{2,1,0:T(8,128)(2,1)S(1)} all-gather(bf16[1,129,128]{2,1,0:T(8,128)(2,1)S(1)} %maximum_bitcast_fusion.1), channel_id=3, replica_groups=mesh['sp_0'=8,'sp_1'=4,'tp'=8] {'sp_0'}, dimensions={0}, use_global_device_ids=true | all-gather | bytes 297216 | tf_op jit(solution)/shard_map/all_gather | solution.py:36
  113.9 1.7 multiply_reduce_fusion.1
  115.7 3.6 %fusion.48 = bf16[1024,128]{1,0:T(8,128)(2,1)S(1)} fusion(bf16[1024,2048]{1,0:T(8,128)(2,1)} %copy-done.1, bf16[2048,128]{1,0:T(8,128)(2,1)S(1)} %copy-done.16, f32[1024,1,128]{2,0,1:T(8,128)S(1)} %get-tuple-element.181, f32[128]{0:T(128)S(1)} %copy-done.18, f32[1024]{0:T(1024)S(1)} %add_rsqrt_fusion.1), kind=kOutput, calls=%fused_computation.81 | convolution fusion | flops 538181632 | bytes 5509632 | tf_op jit(solution)/shard_map/dot_general | solution.py:119
  119.4 1.3 multiply_reduce_fusion
  122.6 34.7 %all_to_all.19 = bf16[256,8,256]{0,2,1:T(8,128)(2,1)S(1)} all-to-all(bf16[256,8,256]{0,2,1:T(8,128)(2,1)S(1)} %bitcast.205), channel_id=1, replica_groups=mesh['sp_0'=8,'sp_1'=4,'tp'=8] {'tp'}, dimensions={1} | all-to-all | bytes 2097152 | tf_op jit(solution)/shard_map/all_to_all | solution.py:177
  157.8 16.6 %all-gather.6.cloned.1.call-done = bf16[1024,2048]{1,0:T(8,128)(2,1)} async-done(((bf16[1024,256]{1,0:T(8,128)(2,1)}), bf16[1024,2048]{1,0:T(8,128)(2,1)}) %all-gather.6.cloned.1.call-update) | async-done | bytes 4194320 | tf_op jit(solution)/shard_map/all_gather | solution.py:179
  174.4 4.2 %convolution_convert_fusion = bf16[1024,256]{1,0:T(8,128)(2,1)} fusion(bf16[1024,2048]{1,0:T(8,128)(2,1)} %all-gather.6.cloned.1.call-done, bf16[2048,256]{1,0:T(8,128)(2,1)S(1)} %bitcast.209), kind=kOutput, calls=%fused_computation.48 | convolution fusion | flops 1074003968 | bytes 5767168 | tf_op jit(solution)/shard_map/dot_general | solution.py:178
  (261 shorter events, 34.6 us)
Async XLA Ops:
  6.5 15.5 %copy-start = (bf16[2048,128]{1,0:T(8,128)(2,1)S(1)}, bf16[2048,128]{1,0:T(8,128)(2,1)}, u32[]{:S(2)}) copy-start(bf16[2048,128]{1,0:T(8,128)(2,1)} %param.21) | copy-start | bytes 1572868
  6.5 3.2 %copy-start.9 = (f32[2048]{0:T(1024)S(1)}, f32[2048]{0:T(1024)}, u32[]{:S(2)}) copy-start(f32[2048]{0:T(1024)} %param.19) | copy-start | bytes 24580
  6.5 167.9 %all-gather.6.cloned.1.call-start = ((), (), s32[]{:S(2)}) async-start(), calls=%async_computation.1 | async-start | bytes 4718592 | tf_op jit(solution)/shard_map/all_gather | solution.py:179
  6.5 3.5 %copy-start.4 = (bf16[1024,2048]{1,0:T(8,128)(2,1)S(1)}, bf16[1024,2048]{1,0:T(8,128)(2,1)}, u32[]{:S(2)}) copy-start(bf16[1024,2048]{1,0:T(8,128)(2,1)} %param.18) | copy-start | bytes 12582916
  10.1 1.0 copy-start.5
  11.1 2.7 %copy-start.1 = (bf16[1024,2048]{1,0:T(8,128)(2,1)}, bf16[1024,2048]{1,0:T(8,128)(2,1)S(1)}, u32[]{:S(2)}) copy-start(bf16[1024,2048]{1,0:T(8,128)(2,1)S(1)} %fusion.32) | copy-start | bytes 12582916
  11.1 1.4 copy-start.6
  12.5 4.6 %copy-start.11 = (f32[128]{0:T(128)S(1)}, f32[128]{0:T(128)}, u32[]{:S(2)}) copy-start(f32[128]{0:T(128)} %param.27) | copy-start | bytes 1540
  12.5 4.6 %copy-start.13 = (bf16[2048,128]{1,0:T(8,128)(2,1)S(1)}, bf16[2048,128]{1,0:T(8,128)(2,1)}, u32[]{:S(2)}) copy-start(bf16[2048,128]{1,0:T(8,128)(2,1)} %param.20) | copy-start | bytes 1572868
  13.8 105.5 %collective-permute-start = (bf16[2,128]{1,0:T(2,128)(2,1)S(1)}, bf16[2,128]{1,0:T(2,128)(2,1)S(1)}, u32[]{:S(2)}, u32[]{:S(2)}) collective-permute-start(bf16[2,128]{1,0:T(2,128)(2,1)S(1)} %slice.193), channel_id=1, source_target_pairs={{0,8},{8,16},{16,24},{24,32},{32,40},{40,48},{48,56},{56,64},{64,7... | collective-permute-start | bytes 1544 | tf_op jit(solution)/shard_map/ppermute | solution.py:19
  17.1 3.6 %copy-start.2 = (bf16[1024,2048]{1,0:T(8,128)(2,1)S(1)}, bf16[1024,2048]{1,0:T(8,128)(2,1)}, u32[]{:S(2)}) copy-start(bf16[1024,2048]{1,0:T(8,128)(2,1)} %copy-done.1) | copy-start | bytes 12582916
  17.1 3.6 %copy-start.14 = (bf16[2048,128]{1,0:T(8,128)(2,1)S(1)}, bf16[2048,128]{1,0:T(8,128)(2,1)}, u32[]{:S(2)}) copy-start(bf16[2048,128]{1,0:T(8,128)(2,1)} %param.22) | copy-start | bytes 1572868
  20.8 1.3 copy-start.15
  82.5 33.1 %copy-start.10 = (bf16[3,128]{1,0:T(4,128)(2,1)S(1)}, bf16[3,128]{1,0:T(4,128)(2,1)}, u32[]{:S(2)}) copy-start(bf16[3,128]{1,0:T(4,128)(2,1)} %param.30) | copy-start | bytes 2308
  82.5 33.1 %copy-start.16 = (bf16[2048,128]{1,0:T(8,128)(2,1)S(1)}, bf16[2048,128]{1,0:T(8,128)(2,1)}, u32[]{:S(2)}) copy-start(bf16[2048,128]{1,0:T(8,128)(2,1)} %param.23) | copy-start | bytes 1572868
  82.6 33.1 %copy-start.18 = (f32[128]{0:T(128)S(1)}, f32[128]{0:T(128)}, u32[]{:S(2)}) copy-start(f32[128]{0:T(128)} %param.29) | copy-start | bytes 1540
  115.7 3.7 %copy-start.3 = (bf16[1024,2048]{1,0:T(8,128)(2,1)S(1)}, bf16[1024,2048]{1,0:T(8,128)(2,1)}, u32[]{:S(2)}) copy-start(bf16[1024,2048]{1,0:T(8,128)(2,1)} %copy-done.1) | copy-start | bytes 12582916
  115.7 3.7 %copy-start.17 = (bf16[2048,128]{1,0:T(8,128)(2,1)S(1)}, bf16[2048,128]{1,0:T(8,128)(2,1)}, u32[]{:S(2)}) copy-start(bf16[2048,128]{1,0:T(8,128)(2,1)} %param.25) | copy-start | bytes 1572868
  119.4 1.4 copy-start.12
  119.4 2.5 %copy-start.7 = (bf16[128,2048]{1,0:T(8,128)(2,1)S(1)}, bf16[128,2048]{1,0:T(8,128)(2,1)}, u32[]{:S(2)}) copy-start(bf16[128,2048]{1,0:T(8,128)(2,1)} %param.32) | copy-start | bytes 1572868
  119.4 2.7 %copy-start.8 = (bf16[128,2048]{1,0:T(8,128)(2,1)S(1)}, bf16[128,2048]{1,0:T(8,128)(2,1)}, u32[]{:S(2)}) copy-start(bf16[128,2048]{1,0:T(8,128)(2,1)} %param.33) | copy-start | bytes 1572868
Sparse Core Ops, SparseCore 0:
  122.0 52.3 all-gather.5
where the time goes:
time: 187 us; the launch traced here: 185 us
  blocking collectives  65.6 us (35%)
  other arithmetic  44.8 us (24%)
  matrix products  38.1 us (20%)
  waiting for transfers between devices  16.6 us (9%)
  between operations  13.9 us (7%)
  starting transfers between devices  3.21 us (2%)
  local copies, waits for them, and re-layouts  2.2 us (1%)
    all_to_all x1, blocking collectives, body(): lax.all_to_all(weight_rows, 'tp', split_axis=1, concat_axis=0, tiled=True)  34.7 us
    all_gather x2, blocking collectives, collected_together(): both, at, found = (lax.all_gather(jnp.concatenate(lines), axis), 0, {})  30.9 us
    dot_general x16, other arithmetic, state_block(): scores = jnp.einsum('hid,hjd,hijd->hij', query_blk, key_blk, decay_all)  27.3 us
    all_gather x1, waiting for transfers between devices, body(): lax.all_gather(mixed_here, 'tp', axis=1, tiled=True)  16.6 us
    dot_general x7, matrix products, project(): jnp.dot(normed, weight, preferred_element_type=jnp.float32)  14 us
    dot_general x16, matrix products, state_block(): result = carried + jnp.einsum('hij,hje->hie', scores, value_blk)  12.7 us
    exp x16, other arithmetic, state_block(): decay_all = jnp.exp(jnp.where(causal, diff_log, -jnp.inf))  9.79 us
    dot_general x1, matrix products, body(): jnp.dot(lax.all_gather(mixed_here, 'tp', axis=1, tiled=True), columns, pr...  4.24 us
  transfers between devices with their start and end apart: 2, of which 1 were waited for; matrix products, arithmetic and copies ran while one was open for 38% of the time, Pallas kernels for 0%

commit v1 on v0

v1 whole, which is shorter than its diff:
```python
import functools

import jax
import jax.numpy as jnp
from jax import lax
from jax.experimental import pallas as pl
from jax.experimental.pallas import tpu as pltpu
from jax.sharding import Mesh
from jax.sharding import PartitionSpec as P

F = 128
CH = 128
RB = 256
EPS = 1e-6
MESH = pl.DeviceIdType.MESH
F32, BF16 = jnp.float32, jnp.bfloat16
NT = (((1,), (1,)), ((), ()))
TN = (((0,), (0,)), ((), ()))


def mm(a, b):
    return jnp.dot(a, b, preferred_element_type=F32)


def mmg(a, b, dims):
    return lax.dot_general(a, b, dims, preferred_element_type=F32)


def silu(v):
    return v * jax.nn.sigmoid(v)


def kernel(
    NZ, NY, NX, T, D,
    tok_h, gain_h, wq_h, wf_h, wi_h, wo_h, wh_h, wb_h, wc_h, floor_h, leak_h, sgain_h, taps_h, ggain_h, ost_h, ocv_h,
    out,
    tok, xg, wfv, whc, wqo, wb, gain, floor, sgain, ggain, taps, leak, ost, ocv,
    rs, fbuf, km, vb, lbuf, sst, lst, qg, ol, gate, cpad, bproj,
    my, ry, mz, rz, mb, sin, rim, act, g, w, acc, osw,
    ld, ys, yr, zs, zr, bs, br, rms, rmr, as_, ar, rls, rlr, sbs, sbr, wss, wsr, wfs, wfr, oss, osr,
):
    z, y, x, c = (lax.axis_index(a) for a in ("z", "y", "x", "c"))
    H = T // 2
    nb, nc = T // RB, T // CH
    N = D // NX
    KC = 2 * F

    def rcopy(src, dst, ss, rsem, dev):
        return pltpu.make_async_remote_copy(
            src_ref=src, dst_ref=dst, send_sem=ss, recv_sem=rsem, device_id=dev, device_id_type=MESH
        )

    def arrived(dst, sem):
        rcopy(dst, dst, sem, sem, {"c": 1 - c}).wait_recv()

    def left(src, sem):
        rcopy(src, src, sem, sem, {"c": 1 - c}).wait_send()

    nxt_y = lax.rem(y + 1, NY)
    nxt_z = lax.rem(z + (y + 1) // NY, NZ)
    prv_y = lax.rem(y + NY - 1, NY)
    prv_z = lax.rem(z + NZ - (NY - y) // NY, NZ)
    nxt = {"z": nxt_z, "y": nxt_y}
    prv = {"z": prv_z, "y": prv_y}
    other = 1 - c

    bar = pltpu.get_barrier_semaphore()
    count = 0
    for d in range(1, NX):
        for e in range(2):
            pl.semaphore_signal(bar, inc=1, device_id={"x": lax.rem(x + d, NX), "c": e}, device_id_type=MESH)
            count += 1
    pl.semaphore_signal(bar, inc=1, device_id={"c": other}, device_id_type=MESH)
    for d in range(1, NY):
        pl.semaphore_signal(bar, inc=1, device_id={"y": lax.rem(y + d, NY)}, device_id_type=MESH)
    for d in range(1, NZ):
        pl.semaphore_signal(bar, inc=1, device_id={"z": lax.rem(z + d, NZ)}, device_id_type=MESH)
    pl.semaphore_signal(bar, inc=1, device_id=nxt, device_id_type=MESH)
    pl.semaphore_signal(bar, inc=1, device_id=prv, device_id_type=MESH)
    count += 1 + (NY - 1) + (NZ - 1) + 2

    lds = {}

    def load(name, src, dst):
        cp = pltpu.make_async_copy(src, dst, ld.at[len(lds)])
        lds[name] = cp
        cp.start()

    def need(*names):
        for name in names:
            lds[name].wait()

    def rows(i, n):
        return pl.ds(i * n, n)

    load("gain", gain_h, gain)
    load("t0", tok_h.at[rows(0, RB)], tok.at[rows(0, RB)])
    load("wf", wf_h, wfv.at[:, 0:F])
    load("wi", wi_h, wfv.at[:, F : 2 * F])
    for i in range(1, nb):
        load(f"t{i}", tok_h.at[rows(i, RB)], tok.at[rows(i, RB)])
    load("floor", floor_h, floor)
    load("leak", leak_h, leak)
    load("ocv", ocv_h, ocv)
    load("ost", ost_h, ost)

    def prep(i):
        r = rows(i, RB)
        for k in range(RB // 64):
            q = pl.ds(i * RB + k * 64, 64)
            t = tok[q, :].astype(F32)
            xg[q, :] = (t * gain[...]).astype(BF16)
            ms = jnp.sum(t * t, axis=-1, keepdims=True) * (1.0 / D)
            rs[q, :] = jnp.broadcast_to(lax.rsqrt(ms + EPS), (64, F))

    def fv(i):
        r = rows(i, RB)
        p = mm(xg[r, :], wfv[...])
        s = rs[r, :]
        fbuf[r, :] = p[:, 0:F] * s
        vb[r, :] = (p[:, F : 2 * F] * s).astype(BF16)

    ri = lax.broadcasted_iota(jnp.int32, (CH, CH), 0)
    ci = lax.broadcasted_iota(jnp.int32, (CH, CH), 1)
    causal = ri >= ci
    tri = jnp.where(causal, 1.0, 0.0).astype(BF16)

    def block(i, state, start):
        r = rows(i, CH)
        k = (1.0 - floor[...]) * jax.nn.sigmoid(-fbuf[r, :])
        lf = jnp.log1p(-k) + leak[r, :]
        hi = lf.astype(BF16)
        lo = (lf - hi.astype(F32)).astype(BF16)
        two = mm(tri, jnp.concatenate([hi, lo], axis=1))
        cum = two[:, 0:F] + two[:, F : 2 * F]
        total = cum[CH - 1 : CH, :]
        mid = cum[CH // 2 - 1 : CH // 2, :]
        lbuf[r, :] = cum
        lst[i] = jnp.broadcast_to(start, (8, F))
        km[r, :] = (k * jnp.exp(mid - cum)).astype(BF16)
        kd = (k * jnp.exp(total - cum)).astype(BF16)
        sst[i] = state.astype(BF16)
        state = state * jnp.exp(total) + mmg(vb[r, :], kd, TN)
        return state, start + total

    state, start = jnp.zeros((F, F), F32), jnp.zeros((1, F), F32)
    need("gain", "t0")
    prep(0)
    need("wf", "wi")
    per = RB // CH
    for i in range(nb):
        if i + 1 < nb:
            need(f"t{i + 1}")
        if i == 0:
            load("wh", wh_h, whc.at[:, 0:F])
            load("wc", wc_h, whc.at[:, F : 2 * F])
            load("wb", wb_h, wb)
            load("taps", taps_h, taps)
            load("ggain", ggain_h, ggain)
            load("wq", wq_h, wqo.at[:, 0:F])
            load("wo", wo_h, wqo.at[:, F : 2 * F])
            load("sgain", sgain_h, sgain)
        if i == 1:
            need("floor", "leak")
        fv(i)
        if i + 1 < nb:
            prep(i + 1)
        if i >= 1:
            for j in range((i - 1) * per, i * per):
                state, start = block(j, state, start)
        if i == 1:
            need("ocv", "ost")
            pl.semaphore_wait(bar, count)
            for kind, src in ((0, ocv), (1, ost)):
                place = lambda slot: w.at[pl.ds(kind * NX * KC + slot * KC + c * F, F), :]
                for d, slot in ((1, 1), (NX - 1, 2), (2, 3)):
                    to = lax.rem(x + d, NX)
                    rcopy(
                        src.at[:, pl.ds(pl.multiple_of(to * N, N), N)], place(slot),
                        wss.at[kind, slot], wsr.at[kind, slot], {"x": to},
                    ).start()
                mine = src.at[:, pl.ds(pl.multiple_of(x * N, N), N)]
                rcopy(mine, place(0), wfs.at[kind, 0], wfr.at[kind, 0], {"c": other}).start()
                w[pl.ds(pl.multiple_of(kind * NX * KC + c * F, F), F), :] = src[:, pl.ds(pl.multiple_of(x * N, N), N)]
    for j in range((nb - 1) * per, nc):
        state, start = block(j, state, start)

    Q = F // NY
    r16 = lax.broadcasted_iota(jnp.int32, (16, F), 0)

    def decay_rows(dec):
        top = dec.astype(BF16)
        low = (dec - top.astype(F32)).astype(BF16)
        return jnp.where(r16 == 0, top.astype(F32), low.astype(F32)).astype(BF16)

    drow = decay_rows(jnp.exp(start))
    for q in range(NY):
        my[q, 0:Q, :] = state[q * Q : (q + 1) * Q, :].astype(BF16)
        my[q, Q : Q + 16, :] = drow
    ry[y] = my[y]
    for d in range(1, NY):
        to = lax.rem(y + d, NY)
        rcopy(my.at[to], ry.at[y], ys.at[d], yr.at[d], {"y": to}).start()

    need("wh", "wc", "wb", "taps", "ggain")

    def hcb(i):
        r = rows(i, RB)
        s = rs[r, :]
        p = mm(xg[r, :], whc[...])
        cpad[pl.ds(8 + i * RB, RB), :] = ((p[:, 0:F] * s) * (p[:, F : 2 * F] * s)).astype(BF16).astype(F32)
        bproj[r, :] = mm(xg[r, :], wb[...]) * s

    hcb(nb - 1)
    rcopy(cpad.at[pl.ds(T, 8), :], rim, rms.at[0], rmr.at[0], nxt).start()
    for i in range(nb - 2, -1, -1):
        hcb(i)

    tf = taps[...].astype(F32)

    def conv(i):
        r = rows(i, RB)
        total = tf[0:1, :] * cpad[pl.ds(6 + i * RB, RB), :]
        total = total + tf[1:2, :] * cpad[pl.ds(7 + i * RB, RB), :]
        total = total + tf[2:3, :] * cpad[pl.ds(8 + i * RB, RB), :]
        v = bproj[r, :] * total
        ms = jnp.mean(v * v, axis=-1, keepdims=True)
        act[0, r, :] = (v * lax.rsqrt(ms + EPS) * ggain[...]).astype(BF16)

    for i in range(nb - 1, 0, -1):
        conv(i)

    def part(ref, k):
        dec = ref[k, Q : Q + 16, :].astype(F32)
        return ref[k, 0:Q, :].astype(F32), dec[0:1, :] + dec[1:2, :]

    for d in range(1, NY):
        arrived(ry.at[0], yr.at[d])
    ps, pd = [jnp.zeros((Q, F), F32)], [jnp.ones((1, F), F32)]
    for k in range(NY):
        s, dec = part(ry, k)
        ps.append(ps[k] * dec + s)
        pd.append(pd[k] * dec)
    mz[0:Q, :] = ps[NY].astype(BF16)
    mz[Q : Q + 16, :] = decay_rows(pd[NY])
    rz[z] = mz[...]
    for d in range(1, NZ):
        to = lax.rem(z + d, NZ)
        rcopy(mz, rz.at[z], zs.at[d], zr.at[d], {"z": to}).start()

    arrived(rim, rmr.at[0])
    cpad[0:8, :] = jnp.where(z + y == 0, 0.0, rim[...])
    conv(0)

    def gcol(kind, slot):
        return kind * NX * KC + slot * KC

    def spread(kind):
        for k in range(2):
            for way in range(2):
                part_k = k if way == 0 else 1 - k
                to = lax.rem(x + (1 if way == 0 else NX - 1), NX)
                for e in range(2):
                    rcopy(
                        act.at[kind, pl.ds(e * H + part_k * RB, RB), :],
                        g.at[pl.ds(part_k * RB, RB), pl.ds(pl.multiple_of(gcol(kind, 1 + way) + c * F, F), F)],
                        as_.at[kind, way, part_k, e], ar.at[kind, way, part_k, c], {"x": to, "c": e},
                    ).start()
            if k == 0:
                rcopy(
                    act.at[kind, pl.ds(pl.multiple_of(other * H, H), H), :],
                    g.at[:, pl.ds(pl.multiple_of(gcol(kind, 0) + c * F, F), F)],
                    sbs.at[kind], sbr.at[kind], {"c": other},
                ).start()
        g[:, pl.ds(pl.multiple_of(gcol(kind, 0) + c * F, F), F)] = act[kind, pl.ds(pl.multiple_of(c * H, H), H), :]

    def gblock(kind, slot, part_k, e):
        return g.at[pl.ds(part_k * RB, RB), pl.ds(gcol(kind, slot) + e * F, F)]

    def relayed(kind, way):
        part_k = way
        to = lax.rem(x + (1 if way == 0 else NX - 1), NX)
        for e in range(2):
            arrived(gblock(kind, 1 + way, part_k, e), ar.at[kind, way, part_k, e])
        rcopy(
            g.at[pl.ds(part_k * RB, RB), pl.ds(gcol(kind, 1 + way), KC)],
            g.at[pl.ds(part_k * RB, RB), pl.ds(gcol(kind, 3), KC)],
            rls.at[kind, way], rlr.at[kind, way], {"x": to},
        ).start()

    def gathered_near(kind):
        for way in range(2):
            part_k = 1 - way
            for e in range(2):
                arrived(gblock(kind, 1 + way, part_k, e), ar.at[kind, way, part_k, e])
        arrived(g.at[:, pl.ds(0, F)], sbr.at[kind])

    def gathered_far(kind, way):
        arrived(g.at[pl.ds(way * RB, RB), pl.ds(gcol(kind, 3), KC)], rlr.at[kind, way])

    spread(0)

    need("wq", "wo", "sgain")

    def qo(i):
        r = rows(i, RB)
        s = rs[r, :]
        p = mm(xg[r, :], wqo[...])
        fbuf[r, :] = silu(p[:, 0:F] * s)
        gate[r, :] = silu(p[:, F : 2 * F] * s) * sgain[...]

    def reads(i):
        r = rows(i, CH)
        cum = lbuf[r, :]
        q = fbuf[r, :]
        mid = cum[CH // 2 - 1 : CH // 2, :]
        qm = (q * jnp.exp(cum - mid)).astype(BF16)
        ql = (q * jnp.exp(cum)).astype(BF16)
        qg[r, :] = (q * jnp.exp(cum + lst[i][0:1, :])).astype(BF16)
        scores = jnp.where(causal, mmg(qm, km[r, :], NT), 0.0).astype(BF16)
        ol[r, :] = mm(scores, vb[r, :]) + mmg(ql, sst[i], NT)

    for i in range(nb):
        qo(i)
        if i >= 1:
            for j in range((i - 1) * per, i * per):
                reads(j)
    for j in range((nb - 1) * per, nc):
        reads(j)

    for kind in range(2):
        for slot in range(1, 4):
            place = w.at[pl.ds(kind * NX * KC + slot * KC + c * F, F), :]
            arrived(place, wsr.at[kind, slot])
            rcopy(place, place, wfs.at[kind, slot], wfr.at[kind, slot], {"c": other}).start()

    for d in range(1, NZ):
        arrived(rz.at[0], zr.at[d])
    before = jnp.zeros((Q, F), F32)
    for k in range(NZ - 1):
        s, dec = part(rz, k)
        before = jnp.where(k < z, before * dec + s, before)
    for k in range(NY):
        mb[k] = (before * pd[k] + ps[k]).astype(BF16)
    mine = pl.ds(pl.multiple_of(y * Q, Q), Q)
    sin[mine, :] = mb[y]
    for d in range(1, NY):
        to = lax.rem(y + d, NY)
        rcopy(mb.at[to], sin.at[mine, :], bs.at[d], br.at[d], {"y": to}).start()

    relayed(0, 0)
    relayed(0, 1)

    for d in range(1, NY):
        arrived(sin.at[0:Q, :], br.at[d])

    def finish(i):
        r = rows(i, RB)
        v = ol[r, :] + mmg(qg[r, :], sin[...], NT)
        ms = jnp.mean(v * v, axis=-1, keepdims=True)
        act[1, r, :] = (v * lax.rsqrt(ms + EPS) * gate[r, :]).astype(BF16)

    for i in range(nb):
        finish(i)
    spread(1)

    for kind in range(2):
        for slot in range(4):
            arrived(w.at[pl.ds(0, F), :], wfr.at[kind, slot])
    gathered_near(0)
    for way in range(2):
        gathered_far(0, way)
        r = rows(way, RB)
        acc[r, :] = mm(g[r, 0 : NX * KC], w[0 : NX * KC, :])
    relayed(1, 0)
    relayed(1, 1)
    gathered_near(1)
    for way in range(2):
        r = rows(way, RB)
        acc[r, :] = acc[r, :] + mm(g[r, gcol(1, 0) : gcol(1, 3)], w[gcol(1, 0) : gcol(1, 3), :])
    for way in range(2):
        gathered_far(1, way)
        r = rows(way, RB)
        res = (acc[r, :] + mm(g[r, gcol(1, 3) : gcol(1, 4)], w[gcol(1, 3) : gcol(1, 4), :])).astype(BF16)
        first = res[:, 0 : N // 2]
        second = res[:, N // 2 : N]
        osw[r, :] = jnp.where(c == 0, second.astype(F32), first.astype(F32)).astype(BF16)
        o = pl.ds(pl.multiple_of(c * H + way * RB, RB), RB)
        rcopy(osw.at[r, :], out.at[o, :], oss.at[way], osr.at[way], {"c": other}).start()
        out[o, :] = jnp.where(c == 0, first.astype(F32), second.astype(F32)).astype(BF16)

    for d in range(1, NY):
        left(my.at[0], ys.at[d])
        left(mb.at[0], bs.at[d])
    for d in range(1, NZ):
        left(mz, zs.at[d])
    left(rim, rms.at[0])
    for kind in range(2):
        for way in range(2):
            for k in range(2):
                for e in range(2):
                    left(act.at[kind, 0:RB, :], as_.at[kind, way, k, e])
            left(g.at[0:RB, 0:KC], rls.at[kind, way])
        left(act.at[kind, 0:H, :], sbs.at[kind])
        for slot in range(4):
            if slot:
                left(w.at[0:F, :], wss.at[kind, slot])
            left(w.at[0:F, :], wfs.at[kind, slot])
    for way in range(2):
        left(osw.at[0:RB, :], oss.at[way])
        arrived(out.at[0:RB, :], osr.at[way])


def body(NZ, NY, NX, *args):
    (tokens, in_gain, wq, wf, wi, wo, wh, wb, wc, floor, leak, sgain, taps, ggain, ost, ocv) = args
    T, D = tokens.shape
    N = D // NX
    row = lambda a: a.reshape(1, -1)
    V, S = pltpu.VMEM, pltpu.SemaphoreType.DMA
    nc = T // CH
    Q = F // NY
    scratch = [
        V((T, D), BF16), V((T, D), BF16),
        V((D, 2 * F), BF16), V((D, 2 * F), BF16), V((D, 2 * F), BF16), V((D, F), BF16),
        V((1, D), F32), V((1, F), F32), V((1, F), F32), V((1, F), F32), V((3, F), BF16),
        V((T, F), F32), V((F, D), BF16), V((F, D), BF16),
        V((T, F), F32), V((T, F), F32), V((T, F), BF16), V((T, F), BF16), V((T, F), F32),
        V((nc, F, F), BF16), V((nc, 8, F), F32), V((T, F), BF16), V((T, F), F32), V((T, F), F32),
        V((T + 8, F), F32), V((T, F), F32),
        V((NY, Q + 16, F), BF16), V((NY, Q + 16, F), BF16), V((Q + 16, F), BF16), V((NZ, Q + 16, F), BF16),
        V((NY, Q, F), BF16), V((F, F), BF16), V((8, F), F32), V((2, T, F), BF16),
        V((T // 2, 4 * F * NX), BF16), V((4 * F * NX, N), BF16), V((T // 2, N), F32), V((T // 2, N // 2), BF16),
        S((24,)), S((NY,)), S((NY,)), S((NZ,)), S((NZ,)), S((NY,)), S((NY,)), S((1,)), S((1,)),
        S((2, 2, 2, 2)), S((2, 2, 2, 2)), S((2, 2)), S((2, 2)), S((2,)), S((2,)),
        S((2, 4)), S((2, 4)), S((2, 4)), S((2, 4)), S((2,)), S((2,)),
    ]
    return pl.pallas_call(
        functools.partial(kernel, NZ, NY, NX, T, D),
        name="mixer",
        out_shape=jax.ShapeDtypeStruct((T, N // 2), BF16),
        in_specs=[pl.BlockSpec(memory_space=pl.ANY)] * 16,
        out_specs=pl.BlockSpec(memory_space=pltpu.VMEM),
        scratch_shapes=scratch,
        compiler_params=pltpu.CompilerParams(
            collective_id=0, has_side_effects=True, vmem_limit_bytes=58 * 1024 * 1024
        ),
    )(
        tokens, row(in_gain), wq, wf, wi, wo, wh, wb, wc, row(floor), leak, row(sgain), taps, row(ggain), ost, ocv
    )


def solution(mesh):
    NZ, NY, NX = 8, 4, 4
    split = Mesh(mesh.devices.reshape(NZ, NY, NX, 2), ("z", "y", "x", "c"))
    sp, tp = ("z", "y"), ("x", "c")
    wide = P(None, tp)
    placed = (
        P(sp, None), P(), wide, wide, wide, wide, wide, wide, wide, P(tp), P(sp, tp), P(), wide, P(), P(tp, None), P(tp, None),
    )
    return jax.shard_map(
        functools.partial(body, NZ, NY, NX), mesh=split, in_specs=placed, out_specs=P(sp, tp), check_vma=False
    )
```

time: 187 us -> 46.4 us (0.25)
  the two profiles are of different devices: /device:TPU:33 before, /device:TPU:1 now
where the time goes in v1:
time: 46.4 us; the launch traced here: 46.3 us
  Pallas kernels  44.4 us (96%)
  local copies, waits for them, and re-layouts  1.87 us (4%)
    pallas_call x1, Pallas kernels, body(): pl.pallas_call(functools.partial(kernel, NZ, NY, NX, T, D), name='mixer',...  44.4 us
    unnamed x1, local copies, waits for them, and re-layouts  1.87 us

profile of v1, /device:TPU:1, one launch (start us, length us, event | category | flops | bytes accessed | tf_op | source)
XLA Modules:
  0.0 46.3 jit_solution(8000464823801338251)
XLA Ops:
  0.0 44.4 %mixer.1 = bf16[1024,256]{1,0:T(8,128)(2,1)} custom-call(bf16[1024,2048]{1,0:T(8,128)(2,1)} %tok_h.1, f32[1,2048]{1,0:T(1,128)} %bitcast.4, bf16[2048,128]{1,0:T(8,128)(2,1)} %wq_h.1, bf16[2048,128]{1,0:T(8,128)(2,1)} %wf_h.1, bf16[2048,128]{1,0:T(8,128)(2,1)} %wi_h.1, bf16[2048,128]{1,0:T(8,128)(2,1)} %wo_h.1, bf16[2048,128]{1,0:T(8,128)(2,1)} %wh_h.1, ...), custom_call_target="tpu_custom_call" | custom-call | tf_op jit(solution)/shard_map/mixer/pallas_call | solution.py:437
  44.4 1.9 %copy.18 = bf16[1024,256]{1,0:T(8,128)(2,1)} copy(bf16[1024,256]{1,0:T(8,128)(2,1)} %mixer.1) | data formatting | bytes 1048576

commit v2 on v1

v2 whole, which is shorter than its diff:
```python
import functools

import jax
import jax.numpy as jnp
from jax import lax
from jax.experimental import pallas as pl
from jax.experimental.pallas import tpu as pltpu
from jax.sharding import Mesh
from jax.sharding import PartitionSpec as P

F = 128
CH = 128
RB = 256
EPS = 1e-6
MESH = pl.DeviceIdType.MESH
F32, BF16 = jnp.float32, jnp.bfloat16
NT = (((1,), (1,)), ((), ()))
TN = (((0,), (0,)), ((), ()))


def mm(a, b):
    return jnp.dot(a, b, preferred_element_type=F32)


def mmg(a, b, dims):
    return lax.dot_general(a, b, dims, preferred_element_type=F32)


LOG_TERMS = (1.000000000114827, 0.49999993460512276, 0.33333939010389413, 0.24979093708816186, 0.20339952431978914, 0.13889282460472627, 0.24939632181800545)


def log_part(k):
    p = jnp.full_like(k, LOG_TERMS[-1])
    for term in LOG_TERMS[-2::-1]:
        p = p * k + term
    return p * k


def far_first(n):
    return sorted(range(1, n), key=lambda d: (-min(d, n - d), d))


def silu(v):
    return v * jax.nn.sigmoid(v)


def kernel(
    NZ, NY, NX, T, D,
    tok_h, gain_h, wq_h, wf_h, wi_h, wo_h, wh_h, wb_h, wc_h, floor_h, leak_h, sgain_h, taps_h, ggain_h, ost_h, ocv_h,
    out,
    tok, wfv, wrest, gain, gcol, small, taps, leak, wout,
    rs, fbuf, km, vb, lbuf, sst, lst, qg, ol, gate, cpad, bproj,
    my, ry, mz, rz, mb, sin, rim, act, g, w, acc, osw,
    ld, xr, ar, rlr, sbr, w1r, w2r, w3r, wfr, osr, sends,
):
    z, y, x, c = (lax.axis_index(a) for a in ("z", "y", "x", "c"))
    H = T // 2
    nb, nc = T // RB, T // CH
    N = D // NX
    KC = 2 * F

    def rcopy(src, dst, ss, rsem, dev):
        return pltpu.make_async_remote_copy(
            src_ref=src, dst_ref=dst, send_sem=ss, recv_sem=rsem, device_id=dev, device_id_type=MESH
        )

    def arrived(dst, sem):
        rcopy(dst, dst, sem, sem, {"c": 1 - c}).wait_recv()

    def left(src, sem):
        rcopy(src, src, sem, sem, {"c": 1 - c}).wait_send()

    nxt_y = lax.rem(y + 1, NY)
    nxt_z = lax.rem(z + (y + 1) // NY, NZ)
    prv_y = lax.rem(y + NY - 1, NY)
    prv_z = lax.rem(z + NZ - (NY - y) // NY, NZ)
    nxt = {"z": nxt_z, "y": nxt_y}
    prv = {"z": prv_z, "y": prv_y}
    other = 1 - c
    sent, sent_s, sent_z = sends.at[0], sends.at[1], sends.at[2]

    lds = {}

    def load(name, whole, *pairs):
        sem = ld.at[len(lds)]
        lds[name] = whole, sem
        for src, dst in pairs:
            pltpu.make_async_copy(src, dst, sem).start()

    def need(*names):
        for name in names:
            whole, sem = lds[name]
            pltpu.make_async_copy(whole, whole, sem).wait()

    def rows(i, n):
        return pl.ds(i * n, n)

    def load_rows(i):
        r = rows(i, RB)
        load(f"t{i}", tok.at[r], (tok_h.at[r], tok.at[r]))

    def load_pair(name, ref, left_h, right_h):
        load(name, ref, (left_h, ref.at[:, 0:F]), (right_h, ref.at[:, F : 2 * F]))

    def load_pair(ref, at, left_h, right_h):
        return (left_h, ref.at[:, at : at + F]), (right_h, ref.at[:, at + F : at + 2 * F])

    HALF = pl.ds(T // 2, T // 2)
    load("gain", gain, (gain_h, gain))
    load("t0", tok.at[0:RB], (tok_h.at[0:RB], tok.at[0:RB]))
    load("wfv", wfv, *load_pair(wfv, 0, wf_h, wi_h))
    load("t1", tok.at[RB : 2 * RB], (tok_h.at[RB : 2 * RB], tok.at[RB : 2 * RB]))
    load("small", small, (floor_h, small.at[0]), (sgain_h, small.at[1]), (ggain_h, small.at[2]))
    load("t2", tok.at[HALF], (tok_h.at[HALF], tok.at[HALF]))
    load("leak", leak, (leak_h, leak))
    load("wout", wout, (ocv_h, wout.at[0]), (ost_h, wout.at[1]))

    bar = pltpu.get_barrier_semaphore()
    count = 0
    for d in range(1, NX):
        for e in range(2):
            pl.semaphore_signal(bar, inc=1, device_id={"x": lax.rem(x + d, NX), "c": e}, device_id_type=MESH)
            count += 1
    pl.semaphore_signal(bar, inc=1, device_id={"c": other}, device_id_type=MESH)
    for d in range(1, NY):
        pl.semaphore_signal(bar, inc=1, device_id={"y": lax.rem(y + d, NY)}, device_id_type=MESH)
    for d in range(1, NZ):
        pl.semaphore_signal(bar, inc=1, device_id={"z": lax.rem(z + d, NZ)}, device_id_type=MESH)
    pl.semaphore_signal(bar, inc=1, device_id=nxt, device_id_type=MESH)
    pl.semaphore_signal(bar, inc=1, device_id=prv, device_id_type=MESH)
    count += 1 + (NY - 1) + (NZ - 1) + 2

    def turn_gain():
        for k in range(D // F):
            r = rows(k, F)
            gcol[r, :] = jnp.transpose(jnp.broadcast_to(gain[:, k * F : (k + 1) * F], (F, F)))

    def scale(ref):
        for k in range(D // F):
            r = rows(k, F)
            for n in range(ref.shape[1] // F):
                v = ref[r, n * F : (n + 1) * F].astype(F32) * gcol[r, :]
                ref[r, n * F : (n + 1) * F] = v.astype(BF16)

    def norms(i):
        for k in range(RB // 64):
            q = pl.ds(i * RB + k * 64, 64)
            t = tok[q, :].astype(F32)
            ms = jnp.sum(t * t, axis=-1, keepdims=True) * (1.0 / D)
            rs[q, :] = jnp.broadcast_to(lax.rsqrt(ms + EPS), (64, F))

    def fv(i):
        r = rows(i, T // 2)
        p = mm(tok[r, :], wfv[...])
        s = rs[r, :]
        fbuf[r, :] = p[:, 0:F] * s
        vb[r, :] = (p[:, F : 2 * F] * s).astype(BF16)

    ri = lax.broadcasted_iota(jnp.int32, (CH, CH), 0)
    ci = lax.broadcasted_iota(jnp.int32, (CH, CH), 1)
    causal = ri >= ci
    tri = jnp.where(causal, 1.0, 0.0).astype(BF16)

    def block(i, state, start):
        r = rows(i, CH)
        k = (1.0 - small[0]) * jax.nn.sigmoid(-fbuf[r, :])
        lf = leak[r, :] - log_part(k)
        hi = lf.astype(BF16)
        lo = (lf - hi.astype(F32)).astype(BF16)
        two = mm(tri, jnp.concatenate([hi, lo], axis=1))
        cum = two[:, 0:F] + two[:, F : 2 * F]
        total = cum[CH - 1 : CH, :]
        mid = cum[CH // 2 - 1 : CH // 2, :]
        lbuf[r, :] = cum
        lst[i] = jnp.broadcast_to(start, (8, F))
        kmid = k * jnp.exp(mid - cum)
        km[r, :] = kmid.astype(BF16)
        kd = (kmid * jnp.exp(total - mid)).astype(BF16)
        sst[i] = state.astype(BF16)
        state = state * jnp.exp(total) + mmg(vb[r, :], kd, TN)
        return state, start + total

    state, start = jnp.zeros((F, F), F32), jnp.zeros((1, F), F32)
    Q = F // NY
    wpart = pl.ds(pl.multiple_of(y * Q, Q), Q)
    wmine = pl.ds(pl.multiple_of(c * F + y * Q, Q), Q)
    wcore = pl.ds(pl.multiple_of(c * F, F), F)

    def wspread(kind):
        part_w = w.at[kind, 1:NX, wmine, :]
        for d in (1, NY - 1):
            rcopy(part_w, part_w, sent, w2r.at[kind], {"y": lax.rem(y + d, NY)}).start()

    def wrelay(kind):
        arrived(w.at[kind, 1:NX, 0 : 2 * Q, :], w2r.at[kind])
        for d in (1, NY - 1):
            source = lax.rem(y + NY - d, NY)
            at = c * F + source * Q + (0 if d == 1 else Q // 2)
            part_w = w.at[kind, 1:NX, pl.ds(pl.multiple_of(at, Q // 2), Q // 2), :]
            rcopy(part_w, part_w, sent, w3r.at[kind], {"y": lax.rem(y + d, NY)}).start()

    def wforward(kind):
        arrived(w.at[kind, 1:NX, 0:Q, :], w3r.at[kind])
        part_w = w.at[kind, 1:NX, wcore, :]
        rcopy(part_w, part_w, sent, wfr.at[kind], {"c": other}).start()
    with jax.named_scope("head"):
        need("gain")
        turn_gain()
        need("t0")
        norms(0)
        need("wfv")
        scale(wfv)
        need("t1")
        norms(1)
    per = RB // CH
    with jax.named_scope("first"):
        fv(0)
    need("t2", "small", "leak")
    load("wrest", wrest, *load_pair(wrest, 0, wh_h, wc_h), (wb_h, wrest.at[:, 2 * F : 3 * F]), *load_pair(wrest, 3 * F, wq_h, wo_h))
    load("taps", taps, (taps_h, taps))
    with jax.named_scope("first"):
        norms(2)
        norms(3)
        fv(1)
        for j in range(nc // 2):
            state, start = block(j, state, start)
    with jax.named_scope("barrier_wait"):
        need("wout")
        pl.semaphore_wait(bar, count)
    for kind in range(2):
        for d, slot in ((2, 3), (1, 1), (NX - 1, 2)):
            to = lax.rem(x + d, NX)
            rcopy(
                wout.at[kind, wpart, pl.ds(pl.multiple_of(to * N, N), N)],
                w.at[kind, slot, wmine, :], sent, w1r.at[0], {"x": to},
            ).start()
        own = wout.at[kind, :, pl.ds(pl.multiple_of(x * N, N), N)]
        rcopy(own, w.at[kind, 0, wcore, :], sent, wfr.at[kind], {"c": other}).start()
    with jax.named_scope("last_blocks"):
        for j in range(nc // 2, nc):
            state, start = block(j, state, start)

    r16 = lax.broadcasted_iota(jnp.int32, (16, F), 0)

    def decay_rows(dec):
        top = dec.astype(BF16)
        low = (dec - top.astype(F32)).astype(BF16)
        return jnp.where(r16 == 0, top.astype(F32), low.astype(F32)).astype(BF16)

    drow = decay_rows(jnp.exp(start))
    for q in range(NY):
        my[q, 0:Q, :] = state[q * Q : (q + 1) * Q, :].astype(BF16)
        my[q, Q : Q + 16, :] = drow
    ry[y] = my[y]
    for d in far_first(NY):
        to = lax.rem(y + d, NY)
        rcopy(my.at[to], ry.at[y], sent_s, xr.at[0], {"y": to}).start()

    for kind in range(2):
        w[kind, 0, wcore, :] = wout[kind, :, pl.ds(pl.multiple_of(x * N, N), N)]

    with jax.named_scope("w_wait"):
        need("wrest", "taps")
    scale(wrest.at[:, 0 : 3 * F])

    def hcb(i):
        r = rows(i, RB)
        s = rs[r, :]
        p = mm(tok[r, :], wrest[:, 0 : 2 * F])
        cpad[pl.ds(8 + i * RB, RB), :] = ((p[:, 0:F] * s) * (p[:, F : 2 * F] * s)).astype(BF16).astype(F32)
        bproj[r, :] = mm(tok[r, :], wrest[:, 2 * F : 3 * F]) * s

    hcb(nb - 1)
    rcopy(cpad.at[pl.ds(T, 8), :], rim, sent_s, xr.at[3], nxt).start()
    with jax.named_scope("hcb"):
        for i in range(nb - 2, -1, -1):
            hcb(i)

    tf = taps[...].astype(F32)

    def conv(i):
        r = rows(i, RB)
        total = tf[0:1, :] * cpad[pl.ds(6 + i * RB, RB), :]
        total = total + tf[1:2, :] * cpad[pl.ds(7 + i * RB, RB), :]
        total = total + tf[2:3, :] * cpad[pl.ds(8 + i * RB, RB), :]
        v = bproj[r, :] * total
        ms = jnp.mean(v * v, axis=-1, keepdims=True)
        act[0, r, :] = (v * lax.rsqrt(ms + EPS) * small[2]).astype(BF16)

    with jax.named_scope("conv"):
        for i in range(nb - 1, 0, -1):
            conv(i)

    scale(wrest.at[:, 3 * F : 5 * F])

    def qo(i):
        r = rows(i, RB)
        s = rs[r, :]
        p = mm(tok[r, :], wrest[:, 3 * F : 5 * F])
        fbuf[r, :] = silu(p[:, 0:F] * s)
        gate[r, :] = silu(p[:, F : 2 * F] * s) * small[1]

    def reads(i):
        r = rows(i, CH)
        cum = lbuf[r, :]
        q = fbuf[r, :]
        mid = cum[CH // 2 - 1 : CH // 2, :]
        qmid = q * jnp.exp(cum - mid)
        qm = qmid.astype(BF16)
        ql = (qmid * jnp.exp(mid)).astype(BF16)
        qg[r, :] = (qmid * jnp.exp(mid + lst[i][0:1, :])).astype(BF16)
        scores = jnp.where(causal, mmg(qm, km[r, :], NT), 0.0).astype(BF16)
        ol[r, :] = mm(scores, vb[r, :]) + mmg(ql, sst[i], NT)

    with jax.named_scope("qo"):
        qo(0)
        qo(1)
        for j in range(per):
            reads(j)

    def part(ref, k):
        dec = ref[k, Q : Q + 16, :].astype(F32)
        return ref[k, 0:Q, :].astype(F32), dec[0:1, :] + dec[1:2, :]

    with jax.named_scope("s1_wait"):
        arrived(ry.at[0 : NY - 1], xr.at[0])
    ps, pd = [jnp.zeros((Q, F), F32)], [jnp.ones((1, F), F32)]
    for k in range(NY):
        s, dec = part(ry, k)
        ps.append(ps[k] * dec + s)
        pd.append(pd[k] * dec)
    mz[0:Q, :] = ps[NY].astype(BF16)
    mz[Q : Q + 16, :] = decay_rows(pd[NY])
    for d in far_first(NZ):
        @pl.when(z + d < NZ)
        def _():
            rcopy(mz, rz.at[z], sent_z, xr.at[1], {"z": lax.rem(z + d, NZ)}).start()

    with jax.named_scope("qo"):
        for i in range(2, nb):
            qo(i)
            for j in range((i - 1) * per, i * per):
                reads(j)
        for j in range((nb - 1) * per, nc):
            reads(j)

    with jax.named_scope("wspread"):
        arrived(w.at[0:2, 1:NX, 0:Q, :], w1r.at[0])
        wspread(0)
        wspread(1)

    with jax.named_scope("rim_wait"):
        arrived(rim, xr.at[3])
    cpad[0:8, :] = jnp.where(z + y == 0, 0.0, rim[...])
    conv(0)

    def gat(kind, slot):
        return kind * NX * KC + slot * KC

    def send(kind, way, part_k):
        to = lax.rem(x + (1 if way == 0 else NX - 1), NX)
        for e in range(2):
            rcopy(
                act.at[kind, pl.ds(e * H + part_k * RB, RB), :],
                g.at[pl.ds(part_k * RB, RB), pl.ds(pl.multiple_of(gat(kind, 1 + way) + c * F, F), F)],
                sent, ar.at[kind, way, part_k], {"x": to, "c": e},
            ).start()

    def keep(kind):
        place = g.at[:, pl.ds(pl.multiple_of(gat(kind, 0) + c * F, F), F)]
        rcopy(
            act.at[kind, pl.ds(pl.multiple_of(other * H, H), H), :], place, sent, sbr.at[kind], {"c": other}
        ).start()
        place[...] = act[kind, pl.ds(pl.multiple_of(c * H, H), H), :]

    def gblock(kind, slot, part_k):
        return g.at[pl.ds(part_k * RB, RB), pl.ds(gat(kind, slot), KC)]

    def relayed(kind, way):
        part_k = way
        to = lax.rem(x + (1 if way == 0 else NX - 1), NX)
        arrived(gblock(kind, 1 + way, part_k), ar.at[kind, way, part_k])
        rcopy(
            g.at[pl.ds(part_k * RB, RB), pl.ds(gat(kind, 1 + way), KC)],
            g.at[pl.ds(part_k * RB, RB), pl.ds(gat(kind, 3), KC)],
            sent, rlr.at[kind, way], {"x": to},
        ).start()

    def gathered_near(kind):
        for way in range(2):
            part_k = 1 - way
            arrived(gblock(kind, 1 + way, part_k), ar.at[kind, way, part_k])
        arrived(g.at[:, pl.ds(0, F)], sbr.at[kind])

    def gathered_far(kind, way):
        arrived(g.at[pl.ds(way * RB, RB), pl.ds(gat(kind, 3), KC)], rlr.at[kind, way])

    with jax.named_scope("spread0"):
        send(0, 0, 0)
        send(0, 1, 1)
        send(0, 0, 1)
        send(0, 1, 0)
        keep(0)

    with jax.named_scope("s2_wait"):
        for n in range(1, NZ):
            @pl.when(z == n)
            def _():
                arrived(rz.at[0:n], xr.at[1])
    before = jnp.zeros((Q, F), F32)
    for k in range(NZ - 1):
        s, dec = part(rz, k)
        before = jnp.where(k < z, before * dec + s, before)
    for k in range(NY):
        mb[k] = (before * pd[k] + ps[k]).astype(BF16)
    mine = pl.ds(pl.multiple_of(y * Q, Q), Q)
    sin[mine, :] = mb[y]
    for d in far_first(NY):
        to = lax.rem(y + d, NY)
        rcopy(mb.at[to], sin.at[mine, :], sent_s, xr.at[2], {"y": to}).start()

    with jax.named_scope("wrelay0"):
        wrelay(0)
    with jax.named_scope("relay0"):
        relayed(0, 0)
        relayed(0, 1)

    with jax.named_scope("s3_wait"):
        arrived(sin.at[0 : F - Q, :], xr.at[2])

    def finish(i):
        r = rows(i, RB)
        v = ol[r, :] + mmg(qg[r, :], sin[...], NT)
        ms = jnp.mean(v * v, axis=-1, keepdims=True)
        act[1, r, :] = (v * lax.rsqrt(ms + EPS) * gate[r, :]).astype(BF16)

    with jax.named_scope("finish"):
        finish(0)
        finish(2)
        send(1, 0, 0)
        finish(1)
        finish(3)
        send(1, 1, 1)
        send(1, 0, 1)
        send(1, 1, 0)
        keep(1)

    with jax.named_scope("wfr_near0"):
        wforward(0)
        wrelay(1)
        gathered_near(0)
        arrived(w.at[0, :, 0:F, :], wfr.at[0])
    for way in range(2):
        with jax.named_scope("far0"):
            gathered_far(0, way)
        r = rows(way, RB)
        acc[r, :] = mm(g[r, 0 : NX * KC], w[0].reshape(NX * KC, N))
    with jax.named_scope("relay1"):
        relayed(1, 0)
        relayed(1, 1)
    with jax.named_scope("wforward1"):
        wforward(1)
    with jax.named_scope("near1"):
        gathered_near(1)
        arrived(w.at[1, :, 0:F, :], wfr.at[1])
    for way in range(2):
        r = rows(way, RB)
        acc[r, :] = acc[r, :] + mm(g[r, gat(1, 0) : gat(1, 3)], w[1, 0:3].reshape(3 * KC, N))
    for way in range(2):
        with jax.named_scope("far1"):
            gathered_far(1, way)
        r = rows(way, RB)
        res = (acc[r, :] + mm(g[r, gat(1, 3) : gat(1, 4)], w[1, 3])).astype(BF16)
        first = res[:, 0 : N // 2]
        second = res[:, N // 2 : N]
        osw[r, :] = jnp.where(c == 0, second.astype(F32), first.astype(F32)).astype(BF16)
        o = pl.ds(pl.multiple_of(c * H + way * RB, RB), RB)
        rcopy(osw.at[r, :], out.at[o, :], sent, osr.at[0], {"c": other}).start()
        out[o, :] = jnp.where(c == 0, first.astype(F32), second.astype(F32)).astype(BF16)

    few = ((NY - 1) * (Q + 16) + (NY - 1) * Q) // 2 + 8
    KB64 = 16 * D * 2
    weights = 2 * N * (3 * Q + F + 2 * 3 * Q + 3 * Q + 3 * F)
    values = 2 * F * (8 * RB + 2 * 2 * RB + H) + 2 * RB * (N // 2)
    many = 2 * (weights + values)
    for n in range(1, NZ):
        @pl.when(NZ - 1 - z == n)
        def _():
            left(rz.at[0:n], sent_z)
    left(lbuf.at[0:few], sent_s)
    left(tok.at[0 : many // KB64 * 16], sent)
    with jax.named_scope("swap_wait"):
        arrived(out.at[0:H, :], osr.at[0])


def body(NZ, NY, NX, *args):
    (tokens, in_gain, wq, wf, wi, wo, wh, wb, wc, floor, leak, sgain, taps, ggain, ost, ocv) = args
    T, D = tokens.shape
    N = D // NX
    row = lambda a: a.reshape(1, -1)
    V, S = pltpu.VMEM, pltpu.SemaphoreType.DMA
    nc = T // CH
    Q = F // NY
    scratch = [
        V((T, D), BF16), V((D, 2 * F), BF16), V((D, 5 * F), BF16),
        V((1, D), F32), V((D, F), F32), V((3, 1, F), F32), V((3, F), BF16),
        V((T, F), F32), V((2, F, D), BF16),
        V((T, F), F32), V((T, F), F32), V((T, F), BF16), V((T, F), BF16), V((T, F), F32),
        V((nc, F, F), BF16), V((nc, 8, F), F32), V((T, F), BF16), V((T, F), F32), V((T, F), F32),
        V((T + 8, F), F32), V((T, F), F32),
        V((NY, Q + 16, F), BF16), V((NY, Q + 16, F), BF16), V((Q + 16, F), BF16), V((NZ, Q + 16, F), BF16),
        V((NY, Q, F), BF16), V((F, F), BF16), V((8, F), F32), V((2, T, F), BF16),
        V((T // 2, 4 * F * NX), BF16), V((2, NX, 2 * F, N), BF16), V((T // 2, N), F32), V((T // 2, N // 2), BF16),
        S((10,)), S((4,)), S((2, 2, 2)), S((2, 2)), S((2,)), S((1,)), S((2,)), S((2,)), S((2,)), S((1,)), S((3,)),
    ]
    return pl.pallas_call(
        functools.partial(kernel, NZ, NY, NX, T, D),
        name="mixer",
        out_shape=pltpu.VMEM((T, N // 2), BF16),
        in_specs=[pl.BlockSpec(memory_space=pl.ANY)] * 16,
        out_specs=pl.BlockSpec(memory_space=pltpu.VMEM),
        scratch_shapes=scratch,
        compiler_params=pltpu.CompilerParams(
            collective_id=0, has_side_effects=True, vmem_limit_bytes=58 * 1024 * 1024
        ),
    )(
        tokens, row(in_gain), wq, wf, wi, wo, wh, wb, wc, row(floor), leak, row(sgain), taps, row(ggain), ost, ocv
    )


def solution(mesh):
    NZ, NY, NX = 8, 4, 4
    split = Mesh(mesh.devices.reshape(NZ, NY, NX, 2), ("z", "y", "x", "c"))
    sp, tp = ("z", "y"), ("x", "c")
    wide = P(None, tp)
    placed = (
        P(sp, None), P(), wide, wide, wide, wide, wide, wide, wide, P(tp), P(sp, tp), P(), wide, P(), P(tp, None), P(tp, None),
    )
    return jax.shard_map(
        functools.partial(body, NZ, NY, NX), mesh=split, in_specs=placed, out_specs=P(sp, tp), check_vma=False
    )
```

time: 46.4 us -> 40.1 us (0.86)
  Pallas kernels: 44.4 us -> 39.2 us
  local copies, waits for them, and re-layouts: 1.87 us -> 0.8 us
    pallas_call x1, Pallas kernels: 44.4 us -> 39.2 us  [body(): pl.pallas_call(functools.partial(kernel, NZ, NY, NX, T, D), name='mixer',...]
    unnamed x1, local copies, waits for them, and re-layouts: 1.87 us -> 0.8 us
where the time goes in v2:
time: 40.1 us; the launch traced here: 40 us
  Pallas kernels  39.2 us (98%)
  local copies, waits for them, and re-layouts  0.8 us (2%)
    pallas_call x1, Pallas kernels, body(): pl.pallas_call(functools.partial(kernel, NZ, NY, NX, T, D), name='mixer',...  39.2 us

profile of v2, /device:TPU:1, one launch (start us, length us, event | category | flops | bytes accessed | tf_op | source)
XLA Modules:
  0.0 40.0 jit_solution(422325573557477428)
XLA Ops:
  0.0 39.2 %mixer.1 = bf16[1024,256]{1,0:T(8,128)(2,1)S(1)} custom-call(bf16[1024,2048]{1,0:T(8,128)(2,1)} %tok_h.1, f32[1,2048]{1,0:T(1,128)} %bitcast.4, bf16[2048,128]{1,0:T(8,128)(2,1)} %wq_h.1, bf16[2048,128]{1,0:T(8,128)(2,1)} %wf_h.1, bf16[2048,128]{1,0:T(8,128)(2,1)} %wi_h.1, bf16[2048,128]{1,0:T(8,128)(2,1)} %wo_h.1, bf16[2048,128]{1,0:T(8,128)(2,1)} %wh_h.1, ...), custom_call_target="tpu_custom_call" | custom-call | tf_op jit(solution)/shard_map/mixer/pallas_call | solution.py:516
  39.2 0.8 %copy.18 = bf16[1024,256]{1,0:T(8,128)(2,1)} copy(bf16[1024,256]{1,0:T(8,128)(2,1)S(1)} %mixer.1) | data formatting | bytes 1048576

commit v3 on v2

--- a/solution.py
+++ b/solution.py
@@ -26,7 +26,7 @@
     return lax.dot_general(a, b, dims, preferred_element_type=F32)
 
 
-LOG_TERMS = (1.000000000114827, 0.49999993460512276, 0.33333939010389413, 0.24979093708816186, 0.20339952431978914, 0.13889282460472627, 0.24939632181800545)
+LOG_TERMS = (0.9999999971754615, 0.500001179512937, 0.3332539552536287, 0.25193518431296363, 0.17907403058358232, 0.2660849487304504)
 
 
 def log_part(k):
@@ -50,8 +50,8 @@
     out,
     tok, wfv, wrest, gain, gcol, small, taps, leak, wout,
     rs, fbuf, km, vb, lbuf, sst, lst, qg, ol, gate, cpad, bproj,
-    my, ry, mz, rz, mb, sin, rim, act, g, w, acc, osw,
-    ld, xr, ar, rlr, sbr, w1r, w2r, w3r, wfr, osr, sends,
+    my, ry, mz, rz, mb, pre_s, pre_d, sin, rim, act, g, w, acc, osw,
+    ld, xr, ar, rlr, sbr, w1r, w2r, w3r, wfr, osr, sends, here,
 ):
     z, y, x, c = (lax.axis_index(a) for a in ("z", "y", "x", "c"))
     H = T // 2
@@ -115,20 +115,59 @@
     load("leak", leak, (leak_h, leak))
     load("wout", wout, (ocv_h, wout.at[0]), (ost_h, wout.at[1]))
 
+    ahead = z + y == 0
+    behind = z + y > 0
+
     bar = pltpu.get_barrier_semaphore()
-    count = 0
+
+    def signal(sem, **to):
+        pl.semaphore_signal(sem, inc=1, device_id=to, device_id_type=MESH)
+
     for d in range(1, NX):
         for e in range(2):
-            pl.semaphore_signal(bar, inc=1, device_id={"x": lax.rem(x + d, NX), "c": e}, device_id_type=MESH)
-            count += 1
-    pl.semaphore_signal(bar, inc=1, device_id={"c": other}, device_id_type=MESH)
+            signal(bar, x=lax.rem(x + d, NX), c=e)
+    signal(bar, c=other)
+    near = 2 * (NX - 1) + 1
     for d in range(1, NY):
-        pl.semaphore_signal(bar, inc=1, device_id={"y": lax.rem(y + d, NY)}, device_id_type=MESH)
+        to_y = lax.rem(y + d, NY)
+
+        @pl.when(z + to_y > 0)
+        def _():
+            signal(bar, y=to_y)
+
     for d in range(1, NZ):
-        pl.semaphore_signal(bar, inc=1, device_id={"z": lax.rem(z + d, NZ)}, device_id_type=MESH)
-    pl.semaphore_signal(bar, inc=1, device_id=nxt, device_id_type=MESH)
-    pl.semaphore_signal(bar, inc=1, device_id=prv, device_id_type=MESH)
-    count += 1 + (NY - 1) + (NZ - 1) + 2
+        to_z = lax.rem(z + d, NZ)
+
+        @pl.when(to_z + y > 0)
+        def _():
+            signal(bar, z=to_z)
+
+    @pl.when(nxt_z + nxt_y > 0)
+    def _():
+        signal(bar, **nxt)
+
+    @pl.when(prv_z + prv_y > 0)
+    def _():
+        signal(bar, **prv)
+
+    def meet():
+        need("wout")
+
+        @pl.when(ahead)
+        def _():
+            pl.semaphore_wait(bar, near)
+
+        @pl.when(behind)
+        def _():
+            pl.semaphore_wait(bar, near + (NY - 1) + (NZ - 1) + 2)
+
+        @pl.when(jnp.logical_and(z == 0, y > 0))
+        def _():
+            signal(here.at[0], y=0)
+
+        @pl.when(jnp.logical_and(z > 0, y == 0))
+        def _():
+            signal(here.at[1], z=0)
 
     def turn_gain():
         for k in range(D // F):
@@ -145,8 +184,11 @@
     def norms(i):
         for k in range(RB // 64):
             q = pl.ds(i * RB + k * 64, 64)
-            t = tok[q, :].astype(F32)
-            ms = jnp.sum(t * t, axis=-1, keepdims=True) * (1.0 / D)
+            t = tok[q, :]
+            t = t * t
+            t = t[:, 0 : D // 2] + t[:, D // 2 : D]
+            t = (t[:, 0 : D // 4] + t[:, D // 4 : D // 2]).astype(F32)
+            ms = jnp.sum(t, axis=-1, keepdims=True) * (1.0 / D)
             rs[q, :] = jnp.broadcast_to(lax.rsqrt(ms + EPS), (64, F))
 
     def fv(i):
@@ -203,6 +245,191 @@
         arrived(w.at[kind, 1:NX, 0:Q, :], w3r.at[kind])
         part_w = w.at[kind, 1:NX, wcore, :]
         rcopy(part_w, part_w, sent, wfr.at[kind], {"c": other}).start()
+    def greet():
+        with jax.named_scope("barrier_wait"):
+            meet()
+        for kind in range(2):
+            for d, slot in ((2, 3), (1, 1), (NX - 1, 2)):
+                to = lax.rem(x + d, NX)
+                rcopy(
+                    wout.at[kind, wpart, pl.ds(pl.multiple_of(to * N, N), N)],
+                    w.at[kind, slot, wmine, :], sent, w1r.at[kind], {"x": to},
+                ).start()
+            own = wout.at[kind, :, pl.ds(pl.multiple_of(x * N, N), N)]
+            rcopy(own, w.at[kind, 0, wcore, :], sent, wfr.at[kind], {"c": other}).start()
+
+    r16 = lax.broadcasted_iota(jnp.int32, (16, F), 0)
+
+    def decay_rows(dec):
+        top = dec.astype(BF16)
+        low = (dec - top.astype(F32)).astype(BF16)
+        return jnp.where(r16 == 0, top.astype(F32), low.astype(F32)).astype(BF16)
+
+    def part(ref, k):
+        dec = ref[k, Q : Q + 16, :].astype(F32)
+        return ref[k, 0:Q, :].astype(F32), dec[0:1, :] + dec[1:2, :]
+
+    def first_step():
+        for d in far_first(NY):
+            to = lax.rem(y + d, NY)
+            rcopy(my.at[to], ry.at[y], sent_s, xr.at[0], {"y": to}).start()
+
+    def second_step():
+        with jax.named_scope("s1_wait"):
+            arrived(ry.at[0 : NY - 1], xr.at[0])
+        ps, pd = jnp.zeros((Q, F), F32), jnp.ones((1, F), F32)
+        for k in range(NY):
+            pre_s[k] = ps
+            pre_d[k] = jnp.broadcast_to(pd, (8, F))
+            s, dec = part(ry, k)
+            ps, pd = ps * dec + s, pd * dec
+        @pl.when(ahead)
+        def _():
+            pl.semaphore_wait(here.at[1], NZ - 1)
+
+        mz[0:Q, :] = ps.astype(BF16)
+        mz[Q : Q + 16, :] = decay_rows(pd)
+        for d in far_first(NZ):
+            @pl.when(z + d < NZ)
+            def _():
+                rcopy(mz, rz.at[z], sent_z, xr.at[1], {"z": lax.rem(z + d, NZ)}).start()
+
+    def third_step():
+        with jax.named_scope("s2_wait"):
+            for n in range(1, NZ):
+                @pl.when(z == n)
+                def _():
+                    arrived(rz.at[0:n], xr.at[1])
+        before = jnp.zeros((Q, F), F32)
+        for k in range(NZ - 1):
+            s, dec = part(rz, k)
+            before = jnp.where(k < z, before * dec + s, before)
+        for k in range(NY):
+            mb[k] = (before * pre_d[k][0:1, :] + pre_s[k]).astype(BF16)
+        mine = pl.ds(pl.multiple_of(y * Q, Q), Q)
+        sin[mine, :] = mb[y]
+        for d in far_first(NY):
+            to = lax.rem(y + d, NY)
+            rcopy(mb.at[to], sin.at[mine, :], sent_s, xr.at[2], {"y": to}).start()
+
+    def third_arrived():
+        with jax.named_scope("s3_wait"):
+            arrived(sin.at[0 : F - Q, :], xr.at[2])
+
+    def hcb(i):
+        r = rows(i, RB)
+        s = rs[r, :]
+        p = mm(tok[r, :], wrest[:, 0 : 2 * F])
+        cpad[pl.ds(8 + i * RB, RB), :] = ((p[:, 0:F] * s) * (p[:, F : 2 * F] * s)).astype(BF16).astype(F32)
+        bproj[r, :] = mm(tok[r, :], wrest[:, 2 * F : 3 * F]) * s
+
+    def send_rim():
+        rcopy(cpad.at[pl.ds(T, 8), :], rim, sent_s, xr.at[3], nxt).start()
+
+    def conv(i):
+        tf = taps[...].astype(F32)
+        r = rows(i, RB)
+        total = tf[0:1, :] * cpad[pl.ds(6 + i * RB, RB), :]
+        total = total + tf[1:2, :] * cpad[pl.ds(7 + i * RB, RB), :]
+        total = total + tf[2:3, :] * cpad[pl.ds(8 + i * RB, RB), :]
+        v = bproj[r, :] * total
+        ms = jnp.mean(v * v, axis=-1, keepdims=True)
+        act[0, r, :] = (v * lax.rsqrt(ms + EPS) * small[2]).astype(BF16)
+
+    def qo(i):
+        r = rows(i, RB)
+        s = rs[r, :]
+        p = mm(tok[r, :], wrest[:, 3 * F : 5 * F])
+        fbuf[r, :] = silu(p[:, 0:F] * s)
+        gate[r, :] = silu(p[:, F : 2 * F] * s) * small[1]
+
+    def reads(i):
+        r = rows(i, CH)
+        cum = lbuf[r, :]
+        q = fbuf[r, :]
+        mid = cum[CH // 2 - 1 : CH // 2, :]
+        qmid = q * jnp.exp(cum - mid)
+        qm = qmid.astype(BF16)
+        ql = (qmid * jnp.exp(mid)).astype(BF16)
+        qg[r, :] = (qmid * jnp.exp(mid + lst[i][0:1, :])).astype(BF16)
+        scores = jnp.where(causal, mmg(qm, km[r, :], NT), 0.0).astype(BF16)
+        ol[r, :] = mm(scores, vb[r, :]) + mmg(ql, sst[i], NT)
+
+    def gat(kind, slot):
+        return kind * NX * KC + slot * KC
+
+    def send(kind, way, part_k, e):
+        to = lax.rem(x + (1 if way == 0 else NX - 1), NX)
+        rcopy(
+            act.at[kind, pl.ds(e * H + part_k * RB, RB), :],
+            g.at[pl.ds(part_k * RB, RB), pl.ds(pl.multiple_of(gat(kind, 1 + way) + c * F, F), F)],
+            sent, ar.at[kind, way, part_k], {"x": to, "c": e},
+        ).start()
+
+    def keep(kind):
+        place = g.at[:, pl.ds(pl.multiple_of(gat(kind, 0) + c * F, F), F)]
+        rcopy(
+            act.at[kind, pl.ds(pl.multiple_of(other * H, H), H), :], place, sent, sbr.at[kind], {"c": other}
+        ).start()
+        place[...] = act[kind, pl.ds(pl.multiple_of(c * H, H), H), :]
+
+    def gblock(kind, slot, part_k):
+        return g.at[pl.ds(part_k * RB, RB), pl.ds(gat(kind, slot), KC)]
+
+    def relayed(kind, way):
+        part_k = way
+        to = lax.rem(x + (1 if way == 0 else NX - 1), NX)
+        arrived(gblock(kind, 1 + way, part_k), ar.at[kind, way, part_k])
+        rcopy(
+            g.at[pl.ds(part_k * RB, RB), pl.ds(gat(kind, 1 + way), KC)],
+            g.at[pl.ds(part_k * RB, RB), pl.ds(gat(kind, 3), KC)],
+            sent, rlr.at[kind, way], {"x": to},
+        ).start()
+
+    def gathered_near(kind):
+        for way in range(2):
+            part_k = 1 - way
+            arrived(gblock(kind, 1 + way, part_k), ar.at[kind, way, part_k])
+        arrived(g.at[:, pl.ds(0, F)], sbr.at[kind])
+
+    def gathered_far(kind, way):
+        arrived(g.at[pl.ds(way * RB, RB), pl.ds(gat(kind, 3), KC)], rlr.at[kind, way])
+
+    def send_conv():
+        send(0, 1, 1, 0)
+        send(0, 0, 0, 1)
+        send(0, 1, 1, 1)
+        send(0, 0, 1, 0)
+
+    def finish(i, carried):
+        r = rows(i, RB)
+        v = ol[r, :]
+        if carried:
+            v = v + mmg(qg[r, :], sin[...], NT)
+        ms = jnp.mean(v * v, axis=-1, keepdims=True)
+        act[1, r, :] = (v * lax.rsqrt(ms + EPS) * gate[r, :]).astype(BF16)
+
+    def finish_all(carried):
+        with jax.named_scope("finish"):
+            finish(0, carried)
+            finish(2, carried)
+            send(1, 0, 0, 0)
+            send(1, 0, 0, 1)
+            finish(1, carried)
+            finish(3, carried)
+            for e in range(2):
+                send(1, 1, 1, e)
+            for e in range(2):
+                send(1, 0, 1, e)
+            for e in range(2):
+                send(1, 1, 0, e)
+            keep(1)
+
+    def w_near(kind):
+        with jax.named_scope("w_near"):
+            arrived(w.at[kind, 1:NX, 0:Q, :], w1r.at[kind])
+            wspread(kind)
+
     with jax.named_scope("head"):
         need("gain")
         turn_gain()
@@ -224,117 +451,45 @@
         fv(1)
         for j in range(nc // 2):
             state, start = block(j, state, start)
-    with jax.named_scope("barrier_wait"):
-        need("wout")
-        pl.semaphore_wait(bar, count)
-    for kind in range(2):
-        for d, slot in ((2, 3), (1, 1), (NX - 1, 2)):
-            to = lax.rem(x + d, NX)
-            rcopy(
-                wout.at[kind, wpart, pl.ds(pl.multiple_of(to * N, N), N)],
-                w.at[kind, slot, wmine, :], sent, w1r.at[0], {"x": to},
-            ).start()
-        own = wout.at[kind, :, pl.ds(pl.multiple_of(x * N, N), N)]
-        rcopy(own, w.at[kind, 0, wcore, :], sent, wfr.at[kind], {"c": other}).start()
+    greet()
     with jax.named_scope("last_blocks"):
         for j in range(nc // 2, nc):
             state, start = block(j, state, start)
-
-    r16 = lax.broadcasted_iota(jnp.int32, (16, F), 0)
-
-    def decay_rows(dec):
-        top = dec.astype(BF16)
-        low = (dec - top.astype(F32)).astype(BF16)
-        return jnp.where(r16 == 0, top.astype(F32), low.astype(F32)).astype(BF16)
-
     drow = decay_rows(jnp.exp(start))
     for q in range(NY):
         my[q, 0:Q, :] = state[q * Q : (q + 1) * Q, :].astype(BF16)
         my[q, Q : Q + 16, :] = drow
     ry[y] = my[y]
-    for d in far_first(NY):
-        to = lax.rem(y + d, NY)
-        rcopy(my.at[to], ry.at[y], sent_s, xr.at[0], {"y": to}).start()
-
-    for kind in range(2):
-        w[kind, 0, wcore, :] = wout[kind, :, pl.ds(pl.multiple_of(x * N, N), N)]
+    pl.when(behind)(first_step)
 
     with jax.named_scope("w_wait"):
         need("wrest", "taps")
     scale(wrest.at[:, 0 : 3 * F])
-
-    def hcb(i):
-        r = rows(i, RB)
-        s = rs[r, :]
-        p = mm(tok[r, :], wrest[:, 0 : 2 * F])
-        cpad[pl.ds(8 + i * RB, RB), :] = ((p[:, 0:F] * s) * (p[:, F : 2 * F] * s)).astype(BF16).astype(F32)
-        bproj[r, :] = mm(tok[r, :], wrest[:, 2 * F : 3 * F]) * s
-
     hcb(nb - 1)
-    rcopy(cpad.at[pl.ds(T, 8), :], rim, sent_s, xr.at[3], nxt).start()
+    pl.when(behind)(send_rim)
     with jax.named_scope("hcb"):
         for i in range(nb - 2, -1, -1):
             hcb(i)
-
-    tf = taps[...].astype(F32)
-
-    def conv(i):
-        r = rows(i, RB)
-        total = tf[0:1, :] * cpad[pl.ds(6 + i * RB, RB), :]
-        total = total + tf[1:2, :] * cpad[pl.ds(7 + i * RB, RB), :]
-        total = total + tf[2:3, :] * cpad[pl.ds(8 + i * RB, RB), :]
-        v = bproj[r, :] * total
-        ms = jnp.mean(v * v, axis=-1, keepdims=True)
-        act[0, r, :] = (v * lax.rsqrt(ms + EPS) * small[2]).astype(BF16)
-
     with jax.named_scope("conv"):
         for i in range(nb - 1, 0, -1):
             conv(i)
 
-    scale(wrest.at[:, 3 * F : 5 * F])
-
-    def qo(i):
-        r = rows(i, RB)
-        s = rs[r, :]
-        p = mm(tok[r, :], wrest[:, 3 * F : 5 * F])
-        fbuf[r, :] = silu(p[:, 0:F] * s)
-        gate[r, :] = silu(p[:, F : 2 * F] * s) * small[1]
-
-    def reads(i):
-        r = rows(i, CH)
-        cum = lbuf[r, :]
-        q = fbuf[r, :]
-        mid = cum[CH // 2 - 1 : CH // 2, :]
-        qmid = q * jnp.exp(cum - mid)
-        qm = qmid.astype(BF16)
-        ql = (qmid * jnp.exp(mid)).astype(BF16)
-        qg[r, :] = (qmid * jnp.exp(mid + lst[i][0:1, :])).astype(BF16)
-        scores = jnp.where(causal, mmg(qm, km[r, :], NT), 0.0).astype(BF16)
-        ol[r, :] = mm(scores, vb[r, :]) + mmg(ql, sst[i], NT)
+    send_conv()
+
+    @pl.when(behind)
+    def _():
+        w_near(0)
 
     with jax.named_scope("qo"):
+        scale(wrest.at[:, 3 * F : 5 * F])
         qo(0)
         qo(1)
         for j in range(per):
             reads(j)
-
-    def part(ref, k):
-        dec = ref[k, Q : Q + 16, :].astype(F32)
-        return ref[k, 0:Q, :].astype(F32), dec[0:1, :] + dec[1:2, :]
-
-    with jax.named_scope("s1_wait"):
-        arrived(ry.at[0 : NY - 1], xr.at[0])
-    ps, pd = [jnp.zeros((Q, F), F32)], [jnp.ones((1, F), F32)]
-    for k in range(NY):
-        s, dec = part(ry, k)
-        ps.append(ps[k] * dec + s)
-        pd.append(pd[k] * dec)
-    mz[0:Q, :] = ps[NY].astype(BF16)
-    mz[Q : Q + 16, :] = decay_rows(pd[NY])
-    for d in far_first(NZ):
-        @pl.when(z + d < NZ)
-        def _():
-            rcopy(mz, rz.at[z], sent_z, xr.at[1], {"z": lax.rem(z + d, NZ)}).start()
+        for kind in range(2):
+            w[kind, 0, wcore, :] = wout[kind, :, pl.ds(pl.multiple_of(x * N, N), N)]
+
+    pl.when(behind)(second_step)
 
     with jax.named_scope("qo"):
         for i in range(2, nb):
@@ -344,106 +499,46 @@
         for j in range((nb - 1) * per, nc):
             reads(j)
 
-    with jax.named_scope("wspread"):
-        arrived(w.at[0:2, 1:NX, 0:Q, :], w1r.at[0])
-        wspread(0)
-        wspread(1)
-
-    with jax.named_scope("rim_wait"):
-        arrived(rim, xr.at[3])
-    cpad[0:8, :] = jnp.where(z + y == 0, 0.0, rim[...])
-    conv(0)
-
-    def gat(kind, slot):
-        return kind * NX * KC + slot * KC
-
-    def send(kind, way, part_k):
-        to = lax.rem(x + (1 if way == 0 else NX - 1), NX)
-        for e in range(2):
-            rcopy(
-                act.at[kind, pl.ds(e * H + part_k * RB, RB), :],
-                g.at[pl.ds(part_k * RB, RB), pl.ds(pl.multiple_of(gat(kind, 1 + way) + c * F, F), F)],
-                sent, ar.at[kind, way, part_k], {"x": to, "c": e},
-            ).start()
-
-    def keep(kind):
-        place = g.at[:, pl.ds(pl.multiple_of(gat(kind, 0) + c * F, F), F)]
-        rcopy(
-            act.at[kind, pl.ds(pl.multiple_of(other * H, H), H), :], place, sent, sbr.at[kind], {"c": other}
-        ).start()
-        place[...] = act[kind, pl.ds(pl.multiple_of(c * H, H), H), :]
-
-    def gblock(kind, slot, part_k):
-        return g.at[pl.ds(part_k * RB, RB), pl.ds(gat(kind, slot), KC)]
-
-    def relayed(kind, way):
-        part_k = way
-        to = lax.rem(x + (1 if way == 0 else NX - 1), NX)
-        arrived(gblock(kind, 1 + way, part_k), ar.at[kind, way, part_k])
-        rcopy(
-            g.at[pl.ds(part_k * RB, RB), pl.ds(gat(kind, 1 + way), KC)],
-            g.at[pl.ds(part_k * RB, RB), pl.ds(gat(kind, 3), KC)],
-            sent, rlr.at[kind, way], {"x": to},
-        ).start()
-
-    def gathered_near(kind):
-        for way in range(2):
-            part_k = 1 - way
-            arrived(gblock(kind, 1 + way, part_k), ar.at[kind, way, part_k])
-        arrived(g.at[:, pl.ds(0, F)], sbr.at[kind])
-
-    def gathered_far(kind, way):
-        arrived(g.at[pl.ds(way * RB, RB), pl.ds(gat(kind, 3), KC)], rlr.at[kind, way])
+    @pl.when(behind)
+    def _():
+        with jax.named_scope("rim_wait"):
+            arrived(rim, xr.at[3])
+        cpad[0:8, :] = rim[...]
+
+    @pl.when(ahead)
+    def _():
+        cpad[0:8, :] = jnp.zeros((8, F), F32)
 
     with jax.named_scope("spread0"):
-        send(0, 0, 0)
-        send(0, 1, 1)
-        send(0, 0, 1)
-        send(0, 1, 0)
+        conv(0)
+        send(0, 0, 0, 0)
+        send(0, 1, 0, 0)
+        send(0, 0, 1, 1)
+        send(0, 1, 0, 1)
         keep(0)
 
-    with jax.named_scope("s2_wait"):
-        for n in range(1, NZ):
-            @pl.when(z == n)
-            def _():
-                arrived(rz.at[0:n], xr.at[1])
-    before = jnp.zeros((Q, F), F32)
-    for k in range(NZ - 1):
-        s, dec = part(rz, k)
-        before = jnp.where(k < z, before * dec + s, before)
-    for k in range(NY):
-        mb[k] = (before * pd[k] + ps[k]).astype(BF16)
-    mine = pl.ds(pl.multiple_of(y * Q, Q), Q)
-    sin[mine, :] = mb[y]
-    for d in far_first(NY):
-        to = lax.rem(y + d, NY)
-        rcopy(mb.at[to], sin.at[mine, :], sent_s, xr.at[2], {"y": to}).start()
-
+    @pl.when(ahead)
+    def _():
+        finish_all(False)
+        with jax.named_scope("here"):
+            pl.semaphore_wait(here.at[0], NY - 1)
+        first_step()
+        send_rim()
+        second_step()
+        w_near(0)
+
+    third_step()
     with jax.named_scope("wrelay0"):
+        w_near(1)
         wrelay(0)
     with jax.named_scope("relay0"):
         relayed(0, 0)
         relayed(0, 1)
 
-    with jax.named_scope("s3_wait"):
-        arrived(sin.at[0 : F - Q, :], xr.at[2])
-
-    def finish(i):
-        r = rows(i, RB)
-        v = ol[r, :] + mmg(qg[r, :], sin[...], NT)
-        ms = jnp.mean(v * v, axis=-1, keepdims=True)
-        act[1, r, :] = (v * lax.rsqrt(ms + EPS) * gate[r, :]).astype(BF16)
-
-    with jax.named_scope("finish"):
-        finish(0)
-        finish(2)
-        send(1, 0, 0)
-        finish(1)
-        finish(3)
-        send(1, 1, 1)
-        send(1, 0, 1)
-        send(1, 1, 0)
-        keep(1)
+    @pl.when(behind)
+    def _():
+        third_arrived()
+        finish_all(True)
 
     with jax.named_scope("wfr_near0"):
         wforward(0)
@@ -478,6 +573,11 @@
         rcopy(osw.at[r, :], out.at[o, :], sent, osr.at[0], {"c": other}).start()
         out[o, :] = jnp.where(c == 0, first.astype(F32), second.astype(F32)).astype(BF16)
 
+    @pl.when(ahead)
+    def _():
+        arrived(rim, xr.at[3])
+        third_arrived()
+
     few = ((NY - 1) * (Q + 16) + (NY - 1) * Q) // 2 + 8
     KB64 = 16 * D * 2
     weights = 2 * N * (3 * Q + F + 2 * 3 * Q + 3 * Q + 3 * F)
@@ -509,9 +609,9 @@
         V((nc, F, F), BF16), V((nc, 8, F), F32), V((T, F), BF16), V((T, F), F32), V((T, F), F32),
         V((T + 8, F), F32), V((T, F), F32),
         V((NY, Q + 16, F), BF16), V((NY, Q + 16, F), BF16), V((Q + 16, F), BF16), V((NZ, Q + 16, F), BF16),
-        V((NY, Q, F), BF16), V((F, F), BF16), V((8, F), F32), V((2, T, F), BF16),
+        V((NY, Q, F), BF16), V((NY, Q, F), F32), V((NY, 8, F), F32), V((F, F), BF16), V((8, F), F32), V((2, T, F), BF16),
         V((T // 2, 4 * F * NX), BF16), V((2, NX, 2 * F, N), BF16), V((T // 2, N), F32), V((T // 2, N // 2), BF16),
-        S((10,)), S((4,)), S((2, 2, 2)), S((2, 2)), S((2,)), S((1,)), S((2,)), S((2,)), S((2,)), S((1,)), S((3,)),
+        S((10,)), S((4,)), S((2, 2, 2)), S((2, 2)), S((2,)), S((2,)), S((2,)), S((2,)), S((2,)), S((1,)), S((3,)), pltpu.SemaphoreType.REGULAR((2,)),
     ]
     return pl.pallas_call(
         functools.partial(kernel, NZ, NY, NX, T, D),

time: 40.1 us -> 35.5 us (0.89)
  the two profiles are of different devices: /device:TPU:1 before, /device:TPU:9 now
where the time goes in v3:
time: 35.5 us; the launch traced here: 35.4 us
  Pallas kernels  34.6 us (97%)
  local copies, waits for them, and re-layouts  0.8 us (2%)
    pallas_call x1, Pallas kernels, body(): pl.pallas_call(functools.partial(kernel, NZ, NY, NX, T, D), name='mixer',...  34.6 us
    unnamed x1, local copies, waits for them, and re-layouts  0.8 us

profile of v3, /device:TPU:9, one launch (start us, length us, event | category | flops | bytes accessed | tf_op | source)
XLA Modules:
  0.0 35.4 jit_solution(8574221680302202104)
XLA Ops:
  0.0 34.6 %mixer.1 = bf16[1024,256]{1,0:T(8,128)(2,1)S(1)} custom-call(bf16[1024,2048]{1,0:T(8,128)(2,1)} %tok_h.1, f32[1,2048]{1,0:T(1,128)} %bitcast.4, bf16[2048,128]{1,0:T(8,128)(2,1)} %wq_h.1, bf16[2048,128]{1,0:T(8,128)(2,1)} %wf_h.1, bf16[2048,128]{1,0:T(8,128)(2,1)} %wi_h.1, bf16[2048,128]{1,0:T(8,128)(2,1)} %wo_h.1, bf16[2048,128]{1,0:T(8,128)(2,1)} %wh_h.1, ...), custom_call_target="tpu_custom_call" | custom-call | tf_op jit(solution)/shard_map/mixer/pallas_call | solution.py:616
  34.6 0.8 %copy.18 = bf16[1024,256]{1,0:T(8,128)(2,1)} copy(bf16[1024,256]{1,0:T(8,128)(2,1)S(1)} %mixer.1) | data formatting | bytes 1048576
